TPU v7x, 256 devices: a whole 4x4x8 slice. The times are simulated.
256 devices in a mesh: ra: 32 (over z, y), cb: 8 (over x, core).
Axes of the slice: x: 4, y: 4, z: 8, core: 2. Of those that a mesh axis runs over, the one named last changes fastest.
Arguments:
- tokens: bfloat16 [128, 2048], P(None, 'ra'), may hold values from -6 to 6
- pre_gain: float32 [2, 2048], P(None, 'ra'), may hold values from 0.1 to 1.9
- post_gain: float32 [2, 2048], P(None, 'ra'), may hold values from 0.1 to 1.9
- gate_weight: bfloat16 [2, 2048, 5632], P(None, 'ra', 'cb'), may hold values from -0.125 to 0.125
- up_weight: bfloat16 [2, 2048, 5632], P(None, 'ra', 'cb'), may hold values from -0.125 to 0.125
- down_weight: bfloat16 [2, 5632, 2048], P(None, 'cb', 'ra'), may hold values from -0.078125 to 0.078125
Outputs:
- mixed: bfloat16 [128, 2048], P(None, 'ra')
All inputs are finite; a program needn't handle non-finite values.
Results may differ from a plain program's by a relative error of at most 0.008.
Values may be sent and summed in bfloat16 or wider, within the bound.
No kernel may reach another device: no remote copies, remote signals or barrier semaphores. Data moves between devices by JAX's collectives and lax.ppermute only.
A program may use at most 64 MiB of HBM per device.

v0:
```python
import jax
import jax.numpy as jnp
from jax import lax
from jax.experimental import pallas as pl
from jax.experimental.pallas import tpu as pltpu
from jax.sharding import Mesh
from jax.sharding import PartitionSpec as P


D = 2048
EPSILON = 1e-06
RESIDUAL = 0.25
f32 = jnp.float32
bf16 = jnp.bfloat16
RA = ("z", "y_high", "y_low")
PART = ("z", "y_high")
SUM = ("y_low", "cb")


def exchange(tiles, axis):
    return lax.all_to_all(tiles, axis, 0, 0, tiled=True)


def to_all(tile, axis):
    n = lax.axis_size(axis)
    return exchange(jnp.broadcast_to(tile[None], (n, *tile.shape)), axis)


def coded(part):
    top = jnp.maximum(jnp.max(jnp.abs(part), axis=0, keepdims=True), 1e-30)
    power = jnp.floor(jnp.log2(top))
    return jnp.concatenate([part * jnp.exp2(-power), jnp.broadcast_to(power, (8, part.shape[1]))]).astype(jnp.float16)


def decoded(tiles):
    tiles = tiles.astype(f32)
    width = tiles.shape[1] - 8
    return tiles[:, :width] * jnp.exp2(tiles[:, width : width + 1])


def project(weight, columns):
    return lax.dot_general(weight, columns, (((0,), (0,)), ((), ())), preferred_element_type=f32)


def total(sums):
    return jnp.sum(sums, axis=0, keepdims=True)


def column(row):
    k = row.shape[1]
    same = lax.broadcasted_iota(jnp.int32, (k, k), 0) == lax.broadcasted_iota(jnp.int32, (k, k), 1)
    return jnp.sum(jnp.where(same, row, 0.0), axis=1, keepdims=True)


def stacked(columns):
    high = columns.astype(bf16)
    return jnp.concatenate([high, (columns - high.astype(f32)).astype(bf16)], axis=0)


def rows_of(values):
    at = lax.broadcasted_iota(jnp.int32, (8, values[0].shape[1]), 0)
    rows = jnp.zeros((8, values[0].shape[1]), f32)
    for i, value in enumerate(values):
        rows = jnp.where(at == i, value, rows)
    return rows


def multiply(flat_ref, j, weight, columns):
    twice = jnp.concatenate([weight, weight], axis=0)
    flat_ref[j] = lax.dot_general(twice, columns, (((0,), (0,)), ((), ())), preferred_element_type=f32)


def place(flat_ref, stage_ref, last, owners):
    count, width = flat_ref.shape[:2]
    size = width // stage_ref.shape[0]
    for i in owners:
        for j in range(count):
            stage_ref[i, j * size : (j + 1) * size] = flat_ref[j, i * size : (i + 1) * size]
        stage_ref[i, count * size : count * size + last.shape[0]] = last


def gain_lanes(gains):
    lane = lax.broadcasted_iota(jnp.int32, (gains[0].shape[0], 128), 1)
    lanes = jnp.zeros(lane.shape, f32)
    for i, rest in enumerate(gains):
        for k in range(3):
            part = rest.astype(bf16).astype(f32)
            lanes = jnp.where(lane == 3 * i + k, part, lanes)
            rest = rest - part
    return lanes.astype(bf16)


def gain_of(lanes, i):
    lane = lax.broadcasted_iota(jnp.int32, lanes.shape, 1)
    return jnp.sum(jnp.where(lane // 3 == i, lanes.astype(f32), 0.0), axis=1, keepdims=True)


def first_kernel(*refs):
    sources, (out_ref, side_out_ref, flat_ref, stage_ref, tiles_ref, side_ref, *held, in_sems, out_sems) = refs[:5], refs[5:]
    pieces = [*sources[:3], sources[3].at[0], sources[4].at[0]]
    copies = [pltpu.make_async_copy(pieces[i], held[i], in_sems.at[i]) for i in range(5)]
    for copy in copies:
        copy.start()
    tokens_ref, pre_ref, post_ref, gate_ref, up_ref = held
    for copy in copies[:3]:
        copy.wait()
    ntok = tokens_ref.shape[1]
    side_ref[:, :ntok] = tokens_ref[...]
    side_ref[:, ntok:] = gain_lanes([column(row) for row in (pre_ref[1:2], post_ref[0:1], post_ref[1:2])])
    groups = out_sems.shape[0] - 1
    writes = [pltpu.make_async_copy(side_ref, side_out_ref, out_sems.at[groups])]
    writes[0].start()
    start = tokens_ref[...].astype(f32)
    squares = total(start * start)
    high = squares.astype(bf16).astype(f32)
    sums = rows_of([high, squares - high])[:4]
    columns = stacked(start * column(pre_ref[0:1]))
    for k, ref in enumerate((gate_ref, up_ref)):
        copies[3 + k].wait()
        multiply(flat_ref, k, ref[...], columns)
    n = tiles_ref.shape[0]
    for g in range(groups):
        part = slice(g * n // groups, (g + 1) * n // groups)
        place(flat_ref, stage_ref, sums, range(part.start, part.stop))
        tiles_ref[part] = stage_ref[part].astype(bf16)
        writes.append(pltpu.make_async_copy(tiles_ref.at[part], out_ref.at[part], out_sems.at[g]))
        writes[-1].start()
    for write in writes:
        write.wait()


def first_tiles(n, *operands):
    width, ntok = operands[-1].shape[2], operands[0].shape[1]
    rows, groups = 2 * (width // n) + 4, 2
    side = operands[0].shape[0], ntok + 128
    hbm = pl.BlockSpec(memory_space=pltpu.HBM)
    return pl.pallas_call(
        first_kernel,
        out_shape=[jax.ShapeDtypeStruct((n, rows, ntok), bf16), jax.ShapeDtypeStruct(side, bf16)],
        in_specs=[hbm] * 5,
        out_specs=[hbm] * 2,
        scratch_shapes=[
            pltpu.VMEM((2, width, ntok), f32),
            pltpu.VMEM((n, rows, ntok), f32),
            pltpu.VMEM((n, rows, ntok), bf16),
            pltpu.VMEM(side, bf16),
            *[pltpu.VMEM(x.shape, x.dtype) for x in operands[:3]],
            *[pltpu.VMEM(x.shape[1:], x.dtype) for x in operands[3:]],
            pltpu.SemaphoreType.DMA((5,)),
            pltpu.SemaphoreType.DMA((groups + 1,)),
        ],
    )(*operands)


def second_kernel(*refs):
    branch_ref, side_ref, other_ref, weights_ref, out_ref, gained_ref, last_ref, flat_ref, stage_ref = refs
    width, ntok = gained_ref.shape
    held = weights_ref.shape[2]
    other = other_ref.shape[1] - side_ref.shape[1]
    start = jnp.concatenate([side_ref[:, :ntok], other_ref[:, other : other + ntok]]).astype(f32)
    lanes = side_ref[:, ntok:], other_ref[:, other + ntok :]
    gains = [jnp.concatenate([gain_of(part, i) for part in lanes]) for i in range(3)]
    branch = branch_ref[...]
    gained = branch * gains[1]
    gained_ref[...] = gained[:width]
    last_ref[...] = jnp.broadcast_to(gains[2][:width], gained_ref.shape)
    sums = [total(branch * branch), total(gained * gained), total(start * gained)]
    high = [part.astype(bf16).astype(f32) for part in sums]
    sums = rows_of(high + [part - rounded for part, rounded in zip(sums, high)])
    for i, columns in enumerate((gained, start)):
        columns = stacked(columns * gains[0])
        for k in range(2):
            weight = jnp.concatenate([weights_ref[k], other_ref[:, k * other // 2 : k * other // 2 + held]])
            multiply(flat_ref, 2 * i + k, weight, columns)
    place(flat_ref, stage_ref, sums, range(out_ref.shape[0]))
    out_ref[...] = stage_ref[...].astype(bf16)


def second_tiles(n, *operands):
    (width, ntok), held = (operands[1].shape[0], operands[0].shape[1]), operands[-1].shape[2]
    rows = 4 * (held // n) + 8
    vmem = pl.BlockSpec(memory_space=pltpu.VMEM)
    return pl.pallas_call(
        second_kernel,
        out_shape=[jax.ShapeDtypeStruct((n, rows, ntok), bf16), *[jax.ShapeDtypeStruct((width, ntok), f32)] * 2],
        in_specs=[vmem] * len(operands),
        out_specs=[vmem] * 3,
        scratch_shapes=[pltpu.VMEM((4, held, ntok), f32), pltpu.VMEM((n, rows, ntok), f32)],
        compiler_params=pltpu.CompilerParams(vmem_limit_bytes=12 * 2**20),
    )(*operands)


def traded(array):
    return lax.ppermute(array, "y_low", [(0, 1), (1, 0)])


def sublayers(tokens, pre_gain, post_gain, gate_weight, up_weight, down_weight):
    n = lax.axis_size(RA)
    size = gate_weight.shape[2] // n
    turned = tokens.T
    start = turned.astype(f32)
    width, ntok = start.shape
    low = lax.axis_index("y_low") == 0

    def pair(first, second):
        return jnp.where(low, first, second), jnp.where(low, second, first)

    tiles, side = first_tiles(n, turned, pre_gain, post_gain, gate_weight, up_weight)

    held = gate_weight.shape[2] // 2
    weights, given = zip(*[pair(weight[1, :, :held], weight[1, :, held:]) for weight in (gate_weight, up_weight)])
    down, given_down = pair(down_weight[1, :held], down_weight[1, held:])
    given = jnp.concatenate([*[jnp.pad(part, ((0, 0), (0, -held % 128))) for part in given], side], axis=1)
    tiles, weights, given, down, given_down = lax.optimization_barrier(
        (tiles, jnp.stack(weights), given, down, given_down)
    )
    other = traded(given)
    other_down = traded(given_down)
    got = exchange(tiles, RA)
    got = jnp.sum(got.astype(f32), axis=0)
    squares = total(got[2 * size : 2 * size + 2])
    scale_in = lax.rsqrt(squares / D + EPSILON)

    def hidden_of(both, axes):
        hidden = (jax.nn.silu(both[:size]) * both[size:]).astype(bf16)
        return to_all(hidden, axes).reshape(-1, ntok)

    hidden = hidden_of(got[: 2 * size] * scale_in, RA)
    parts = decoded(to_all(coded(project(down_weight[0], hidden)), SUM))
    branch = jnp.concatenate(pair(*jnp.sum(parts.reshape(2, -1, width, ntok), axis=1)))

    tiles, gained, last = second_tiles(n // 2, branch, side, other, weights)
    got = jnp.sum(exchange(tiles, PART).astype(f32), axis=0)
    sums = got[4 * size : 4 * size + 3] + got[4 * size + 3 : 4 * size + 6]
    branch_sq, gained_sq, cross = sums[0:1], sums[1:2], sums[2:3]
    scale_out = lax.rsqrt(branch_sq / D + EPSILON)
    squares = RESIDUAL * RESIDUAL * squares + 2.0 * RESIDUAL * scale_out * cross + scale_out * scale_out * gained_sq
    scale_in = lax.rsqrt(squares / D + EPSILON)
    stream = RESIDUAL * start + gained * scale_out

    both = (RESIDUAL * got[2 * size : 4 * size] + scale_out * got[: 2 * size]) * scale_in
    hidden = hidden_of(both, PART)
    halves = pair(coded(project(down, hidden)), coded(project(other_down, hidden)))
    members = lax.axis_size("cb")
    parts = jnp.concatenate([jnp.broadcast_to(half[None], (members, *half.shape)) for half in halves])
    branch = jnp.sum(decoded(exchange(parts, SUM)), axis=0)
    branch_sq = jnp.sum(to_all(total(branch * branch), RA), axis=0)
    scale_out = lax.rsqrt(branch_sq / D + EPSILON)
    stream = RESIDUAL * stream + branch * last * scale_out
    return stream.astype(bf16).T


def solution(mesh):
    split = Mesh(mesh.devices.reshape(8, 2, 2, mesh.shape["cb"]), ("z", "y_high", "y_low", "cb"))
    return jax.shard_map(
        sublayers,
        mesh=split,
        in_specs=(P(None, RA), P(None, RA), P(None, RA), P(None, RA, "cb"), P(None, RA, "cb"), P(None, "cb", RA)),
        out_specs=P(None, RA),
        check_vma=False,
    )
```

profile of v0, /device:TPU:1, one launch (start us, length us, event | category | flops | bytes accessed | tf_op | source)
XLA Modules:
  0.0 125.0 jit_solution(12375338058002639629)
XLA Ops:
  0.0 0.0 copy-start.1
  0.0 1.0 select_bitcast_fusion
  1.0 0.0 copy-done.1
  1.0 1.0 select_bitcast_fusion.2
  2.0 2.3 %shard_map.64 = (bf16[32,48,128]{2,1,0:T(8,128)(2,1)}, bf16[64,256]{1,0:T(8,128)(2,1)}) custom-call(bf16[64,128]{1,0:T(8,128)(2,1)} %bitcast.46, f32[2,64]{1,0:T(2,128)} %refs_1_.1, f32[2,64]{1,0:T(2,128)} %refs_2_.1, bf16[2,64,704]{2,1,0:T(8,128)(2,1)} %refs_3_.1, bf16[2,64,704]{2,1,0:T(8,128)(2,1)} %refs_4_.1), custom_call_target="tpu_custom_call" | custom-call | tf_op jit(solution)/shard_map/pallas_call | solution.py:137
  4.3 0.8 fusion.5
  5.1 25.9 %all_to_all.35 = bf16[32,48,128]{2,1,0:T(8,128)(2,1)S(1)} all-to-all(bf16[32,48,128]{2,1,0:T(8,128)(2,1)} %get-tuple-element.17), channel_id=1, replica_groups=mesh['z'=8,'y_high'=2,'y_low'=2,'cb'=8] {'z','y_high','y_low'}, dimensions={0} | all-to-all | bytes 786432 | tf_op jit(solution)/shard_map/all_to_all | solution.py:21
  30.9 0.1 convert_reduce_fusion.1
  31.1 14.8 %all_to_all.36 = bf16[32,22,128]{2,1,0:T(8,128)(2,1)S(1)} all-to-all(bf16[32,22,128]{2,1,0:T(8,128)(2,1)S(1)} %broadcast_in_dim.18), channel_id=1, replica_groups=mesh['z'=8,'y_high'=2,'y_low'=2,'cb'=8] {'z','y_high','y_low'}, dimensions={0} | all-to-all | bytes 360448 | tf_op jit(solution)/shard_map/all_to_all | solution.py:21
  45.8 0.0 copy-start.2
  45.8 0.1 reshape.199
  45.9 0.9 copy-done.2
  46.8 0.2 abs_reduce_fusion.2
  47.0 0.7 broadcast_in_dim.20
  47.8 7.4 %all-to-all-start.2 = ((f16[16,72,128]{2,1,0:T(8,128)(2,1)}), f16[16,72,128]{2,1,0:T(8,128)(2,1)S(1)}, u32[]{:S(2)}, u32[]{:S(2)}) async-start(f16[16,72,128]{2,1,0:T(8,128)(2,1)} %broadcast_in_dim.20), calls=%async_computation.2 | async-start | bytes 589824 | tf_op jit(solution)/shard_map/all_to_all | solution.py:21
  55.1 1.4 %collective-permute-start = (bf16[64,1024]{1,0:T(8,128)(2,1)S(1)}, bf16[64,1024]{1,0:T(8,128)(2,1)S(1)}, u32[]{:S(2)}, u32[]{:S(2)}) collective-permute-start(bf16[64,1024]{1,0:T(8,128)(2,1)S(1)} %fusion.5), channel_id=1, source_target_pairs={{0,8},{8,0},{1,9},{9,1},{2,10},{10,2},{3,11},{11,3},{4,12},{12,4},... | collective-permute-start | bytes 393224 | tf_op jit(solution)/shard_map/ppermute | solution.py:194
  56.5 6.1 %all-to-all-done.2 = f16[16,72,128]{2,1,0:T(8,128)(2,1)S(1)} async-done(((f16[16,72,128]{2,1,0:T(8,128)(2,1)}), f16[16,72,128]{2,1,0:T(8,128)(2,1)S(1)}, u32[]{:S(2)}, u32[]{:S(2)}) %all-to-all-start.2) | async-done | bytes 294944 | tf_op jit(solution)/shard_map/all_to_all | solution.py:21
  62.7 0.0 copy-start
  62.8 0.6 collective-permute-done.refs_2_
  63.3 0.2 copy-done
  63.5 0.6 shard_map.65
  64.1 18.1 %all_to_all.37 = bf16[16,96,128]{2,1,0:T(8,128)(2,1)S(1)} all-to-all(bf16[16,96,128]{2,1,0:T(8,128)(2,1)S(1)} %get-tuple-element.21), channel_id=1, replica_groups=mesh['z'=8,'y_high'=2,'y_low'=2,'cb'=8] {'z','y_high'}, dimensions={0} | all-to-all | bytes 786432 | tf_op jit(solution)/shard_map/all_to_all | solution.py:21
  82.2 0.1 convert_reduce_fusion
  82.3 0.6 broadcast_in_dim.21
  83.0 4.3 %all-to-all-start.4 = ((bf16[16,22,128]{2,1,0:T(8,128)(2,1)}), bf16[16,22,128]{2,1,0:T(8,128)(2,1)S(1)}, u32[]{:S(2)}, u32[]{:S(2)}) async-start(bf16[16,22,128]{2,1,0:T(8,128)(2,1)} %broadcast_in_dim.21), calls=%async_computation.4 | async-start | bytes 196608 | tf_op jit(solution)/shard_map/all_to_all | solution.py:21
  87.3 0.3 collective-permute-start.1
  87.6 9.4 %all-to-all-done.4 = bf16[16,22,128]{2,1,0:T(8,128)(2,1)S(1)} async-done(((bf16[16,22,128]{2,1,0:T(8,128)(2,1)}), bf16[16,22,128]{2,1,0:T(8,128)(2,1)S(1)}, u32[]{:S(2)}, u32[]{:S(2)}) %all-to-all-start.4) | async-done | bytes 90144 | tf_op jit(solution)/shard_map/all_to_all | solution.py:21
  97.0 0.2 abs_reduce_fusion.1
  97.2 0.0 collective-permute-done.1
  97.2 0.2 abs_reduce_fusion
  97.5 0.1 pad_maximum_fusion
  97.6 14.3 %all_to_all.38 = f16[16,72,128]{2,1,0:T(8,128)(2,1)S(1)} all-to-all(f16[16,72,128]{2,1,0:T(8,128)(2,1)S(1)} %pad_maximum_fusion), channel_id=1, replica_groups=mesh['z'=8,'y_high'=2,'y_low'=2,'cb'=8] {'y_low','cb'}, dimensions={0} | all-to-all | bytes 589824 | tf_op jit(solution)/shard_map/all_to_all | solution.py:21
  112.0 0.1 fusion
  112.1 11.6 %all_to_all.39 = f32[32,1,128]{2,1,0:T(1,128)S(1)} all-to-all(f32[32,1,128]{2,1,0:T(1,128)S(1)} %broadcast_in_dim.26), channel_id=1, replica_groups=mesh['z'=8,'y_high'=2,'y_low'=2,'cb'=8] {'z','y_high','y_low'}, dimensions={0} | all-to-all | bytes 32768 | tf_op jit(solution)/shard_map/all_to_all | solution.py:21
  123.6 0.0 copy-start.3
  123.7 0.7 copy-done.3
  124.4 0.6 fusion.12
  (35 shorter events, 0.6 us)
Async XLA Ops:
  0.0 1.0 copy-start.1
  45.8 0.9 copy-start.2
  47.8 14.8 %all-to-all-start.2 = ((f16[16,72,128]{2,1,0:T(8,128)(2,1)}), f16[16,72,128]{2,1,0:T(8,128)(2,1)S(1)}, u32[]{:S(2)}, u32[]{:S(2)}) async-start(f16[16,72,128]{2,1,0:T(8,128)(2,1)} %broadcast_in_dim.20), calls=%async_computation.2 | async-start | bytes 589824 | tf_op jit(solution)/shard_map/all_to_all | solution.py:21
  55.1 8.2 %collective-permute-start = (bf16[64,1024]{1,0:T(8,128)(2,1)S(1)}, bf16[64,1024]{1,0:T(8,128)(2,1)S(1)}, u32[]{:S(2)}, u32[]{:S(2)}) collective-permute-start(bf16[64,1024]{1,0:T(8,128)(2,1)S(1)} %fusion.5), channel_id=1, source_target_pairs={{0,8},{8,0},{1,9},{9,1},{2,10},{10,2},{3,11},{11,3},{4,12},{12,4},... | collective-permute-start | bytes 393224 | tf_op jit(solution)/shard_map/ppermute | solution.py:194
  62.7 0.8 copy-start
  83.0 14.0 %all-to-all-start.4 = ((bf16[16,22,128]{2,1,0:T(8,128)(2,1)}), bf16[16,22,128]{2,1,0:T(8,128)(2,1)S(1)}, u32[]{:S(2)}, u32[]{:S(2)}) async-start(bf16[16,22,128]{2,1,0:T(8,128)(2,1)} %broadcast_in_dim.21), calls=%async_computation.4 | async-start | bytes 196608 | tf_op jit(solution)/shard_map/all_to_all | solution.py:21
  87.3 9.9 %collective-permute-start.1 = (bf16[352,64]{0,1:T(8,128)(2,1)S(1)}, bf16[352,64]{0,1:T(8,128)(2,1)S(1)}, u32[]{:S(2)}, u32[]{:S(2)}) collective-permute-start(bf16[352,64]{0,1:T(8,128)(2,1)S(1)} %get-tuple-element.23), channel_id=1, source_target_pairs={{0,8},{8,0},{1,9},{9,1},{2,10},{10,2},{3,11},{11,3},{4,12},{12,4},... | collective-permute-start | bytes 135176 | tf_op jit(solution)/shard_map/ppermute | solution.py:194
  123.6 0.7 copy-start.3
where the time goes:
time: 126 us; the launch traced here: 125 us
  blocking collectives  84.5 us (67%)
  waiting for transfers between devices  16.1 us (13%)
  starting transfers between devices  13.4 us (11%)
  other arithmetic  4.05 us (3%)
  local copies, waits for them, and re-layouts  3.32 us (3%)
  Pallas kernels  2.9 us (2%)
    all_to_all x5, blocking collectives, exchange(): return lax.all_to_all(tiles, axis, 0, 0, tiled=True)  84.5 us
    all_to_all x2, waiting for transfers between devices, exchange(): return lax.all_to_all(tiles, axis, 0, 0, tiled=True)  15.5 us
    all_to_all x2, starting transfers between devices, exchange(): return lax.all_to_all(tiles, axis, 0, 0, tiled=True)  11.7 us
  transfers between devices with their start and end apart: 4, of which 3 were waited for; matrix products, arithmetic and copies ran while one was open for 0% of the time, Pallas kernels for 0%

commit v1 on v0

--- a/solution.py
+++ b/solution.py
@@ -38,8 +38,8 @@
     return tiles[:, :width] * jnp.exp2(tiles[:, width : width + 1])
 
 
-def project(weight, columns):
-    return lax.dot_general(weight, columns, (((0,), (0,)), ((), ())), preferred_element_type=f32)
+def down_project(weight, columns):
+    return jnp.dot(weight, columns, preferred_element_type=f32)
 
 
 def total(sums):
@@ -96,20 +96,15 @@
 
 
 def first_kernel(*refs):
-    sources, (out_ref, side_out_ref, flat_ref, stage_ref, tiles_ref, side_ref, *held, in_sems, out_sems) = refs[:5], refs[5:]
-    pieces = [*sources[:3], sources[3].at[0], sources[4].at[0]]
-    copies = [pltpu.make_async_copy(pieces[i], held[i], in_sems.at[i]) for i in range(5)]
+    sources, (out_ref, keep_out_ref, give_out_ref, *refs) = refs[:6], refs[6:]
+    flat_ref, stage_ref, tiles_ref, keep_ref, give_ref, turn_ref, *held, in_sems, out_sems = refs
+    pieces = [*sources[:3], sources[3].at[0], sources[4].at[0], *[source.at[1] for source in sources[3:]]]
+    copies = [pltpu.make_async_copy(pieces[i], held[i], in_sems.at[i]) for i in range(8)]
     for copy in copies:
         copy.start()
-    tokens_ref, pre_ref, post_ref, gate_ref, up_ref = held
+    tokens_ref, pre_ref, post_ref, gate_ref, up_ref, *traded_refs = held
     for copy in copies[:3]:
         copy.wait()
-    ntok = tokens_ref.shape[1]
-    side_ref[:, :ntok] = tokens_ref[...]
-    side_ref[:, ntok:] = gain_lanes([column(row) for row in (pre_ref[1:2], post_ref[0:1], post_ref[1:2])])
-    groups = out_sems.shape[0] - 1
-    writes = [pltpu.make_async_copy(side_ref, side_out_ref, out_sems.at[groups])]
-    writes[0].start()
     start = tokens_ref[...].astype(f32)
     squares = total(start * start)
     high = squares.astype(bf16).astype(f32)
@@ -118,48 +113,67 @@
     for k, ref in enumerate((gate_ref, up_ref)):
         copies[3 + k].wait()
         multiply(flat_ref, k, ref[...], columns)
-    n = tiles_ref.shape[0]
+    n, groups = tiles_ref.shape[0], out_sems.shape[0] - 2
+    writes = []
     for g in range(groups):
         part = slice(g * n // groups, (g + 1) * n // groups)
         place(flat_ref, stage_ref, sums, range(part.start, part.stop))
         tiles_ref[part] = stage_ref[part].astype(bf16)
         writes.append(pltpu.make_async_copy(tiles_ref.at[part], out_ref.at[part], out_sems.at[g]))
         writes[-1].start()
+
+    low = lax.axis_index("y_low") == 0
+    width, wide = traded_refs[0].shape[1], turn_ref.shape[1]
+    half, step = width // 2, wide // 2
+    for k, ref in enumerate(traded_refs):
+        copies[5 + k].wait()
+        turn_ref[:, :width] = ref[...].astype(f32)
+        first, second = turn_ref[:, :half], pltpu.roll(turn_ref[...], wide - half, 1)[:, :half]
+        keep_ref[:, k * step : k * step + half] = jnp.where(low, first, second).astype(bf16)
+        give_ref[:, k * step : k * step + half] = jnp.where(low, second, first).astype(bf16)
+    ntok = tokens_ref.shape[1]
+    gains = gain_lanes([column(row) for row in (pre_ref[1:2], post_ref[0:1], post_ref[1:2])])
+    for ref in (keep_ref, give_ref):
+        ref[:, 3 * step : 3 * step + ntok] = tokens_ref[...]
+        ref[:, 3 * step + ntok :] = gains
+    for i, (source, target) in enumerate(((keep_ref, keep_out_ref), (give_ref, give_out_ref))):
+        writes.append(pltpu.make_async_copy(source, target, out_sems.at[groups + i]))
+        writes[-1].start()
     for write in writes:
         write.wait()
 
 
 def first_tiles(n, *operands):
-    width, ntok = operands[-1].shape[2], operands[0].shape[1]
-    rows, groups = 2 * (width // n) + 4, 2
-    side = operands[0].shape[0], ntok + 128
+    (count, ntok), width = operands[0].shape, operands[-1].shape[2]
+    rows, groups, step = 2 * (width // n) + 4, 2, -(-width // 256) * 128
+    outs = [jax.ShapeDtypeStruct(shape, bf16) for shape in ((n, rows, ntok), *[(count, 3 * step + ntok + 128)] * 2)]
     hbm = pl.BlockSpec(memory_space=pltpu.HBM)
     return pl.pallas_call(
         first_kernel,
-        out_shape=[jax.ShapeDtypeStruct((n, rows, ntok), bf16), jax.ShapeDtypeStruct(side, bf16)],
-        in_specs=[hbm] * 5,
-        out_specs=[hbm] * 2,
+        out_shape=outs,
+        in_specs=[hbm] * 6,
+        out_specs=[hbm] * 3,
         scratch_shapes=[
             pltpu.VMEM((2, width, ntok), f32),
             pltpu.VMEM((n, rows, ntok), f32),
-            pltpu.VMEM((n, rows, ntok), bf16),
-            pltpu.VMEM(side, bf16),
+            *[pltpu.VMEM(out.shape, bf16) for out in outs],
+            pltpu.VMEM((count, 2 * step), f32),
             *[pltpu.VMEM(x.shape, x.dtype) for x in operands[:3]],
-            *[pltpu.VMEM(x.shape[1:], x.dtype) for x in operands[3:]],
-            pltpu.SemaphoreType.DMA((5,)),
-            pltpu.SemaphoreType.DMA((groups + 1,)),
+            *[pltpu.VMEM((count, width), bf16) for _ in range(5)],
+            pltpu.SemaphoreType.DMA((8,)),
+            pltpu.SemaphoreType.DMA((groups + 2,)),
         ],
     )(*operands)
 
 
 def second_kernel(*refs):
-    branch_ref, side_ref, other_ref, weights_ref, out_ref, gained_ref, last_ref, flat_ref, stage_ref = refs
+    branch_ref, mine_ref, other_ref, out_ref, start_ref, gained_ref, last_ref, flat_ref, stage_ref = refs
     width, ntok = gained_ref.shape
-    held = weights_ref.shape[2]
-    other = other_ref.shape[1] - side_ref.shape[1]
-    start = jnp.concatenate([side_ref[:, :ntok], other_ref[:, other : other + ntok]]).astype(f32)
-    lanes = side_ref[:, ntok:], other_ref[:, other + ntok :]
-    gains = [jnp.concatenate([gain_of(part, i) for part in lanes]) for i in range(3)]
+    held, step = flat_ref.shape[1], (mine_ref.shape[1] - ntok - 128) // 3
+    sides = [ref[:, 3 * step :] for ref in (mine_ref, other_ref)]
+    start = jnp.concatenate([side[:, :ntok] for side in sides]).astype(f32)
+    start_ref[...] = start[:width]
+    gains = [jnp.concatenate([gain_of(side[:, ntok:], i) for side in sides]) for i in range(3)]
     branch = branch_ref[...]
     gained = branch * gains[1]
     gained_ref[...] = gained[:width]
@@ -170,21 +184,21 @@
     for i, columns in enumerate((gained, start)):
         columns = stacked(columns * gains[0])
         for k in range(2):
-            weight = jnp.concatenate([weights_ref[k], other_ref[:, k * other // 2 : k * other // 2 + held]])
+            weight = jnp.concatenate([ref[:, k * step : k * step + held] for ref in (mine_ref, other_ref)])
             multiply(flat_ref, 2 * i + k, weight, columns)
     place(flat_ref, stage_ref, sums, range(out_ref.shape[0]))
     out_ref[...] = stage_ref[...].astype(bf16)
 
 
-def second_tiles(n, *operands):
-    (width, ntok), held = (operands[1].shape[0], operands[0].shape[1]), operands[-1].shape[2]
+def second_tiles(n, held, *operands):
+    width, ntok = operands[1].shape[0], operands[0].shape[1]
     rows = 4 * (held // n) + 8
     vmem = pl.BlockSpec(memory_space=pltpu.VMEM)
     return pl.pallas_call(
         second_kernel,
-        out_shape=[jax.ShapeDtypeStruct((n, rows, ntok), bf16), *[jax.ShapeDtypeStruct((width, ntok), f32)] * 2],
+        out_shape=[jax.ShapeDtypeStruct((n, rows, ntok), bf16), *[jax.ShapeDtypeStruct((width, ntok), f32)] * 3],
         in_specs=[vmem] * len(operands),
-        out_specs=[vmem] * 3,
+        out_specs=[vmem] * 4,
         scratch_shapes=[pltpu.VMEM((4, held, ntok), f32), pltpu.VMEM((n, rows, ntok), f32)],
         compiler_params=pltpu.CompilerParams(vmem_limit_bytes=12 * 2**20),
     )(*operands)
@@ -198,24 +212,17 @@
     n = lax.axis_size(RA)
     size = gate_weight.shape[2] // n
     turned = tokens.T
-    start = turned.astype(f32)
-    width, ntok = start.shape
+    width, ntok = turned.shape
     low = lax.axis_index("y_low") == 0
 
     def pair(first, second):
         return jnp.where(low, first, second), jnp.where(low, second, first)
 
-    tiles, side = first_tiles(n, turned, pre_gain, post_gain, gate_weight, up_weight)
-
     held = gate_weight.shape[2] // 2
-    weights, given = zip(*[pair(weight[1, :, :held], weight[1, :, held:]) for weight in (gate_weight, up_weight)])
-    down, given_down = pair(down_weight[1, :held], down_weight[1, held:])
-    given = jnp.concatenate([*[jnp.pad(part, ((0, 0), (0, -held % 128))) for part in given], side], axis=1)
-    tiles, weights, given, down, given_down = lax.optimization_barrier(
-        (tiles, jnp.stack(weights), given, down, given_down)
-    )
-    other = traded(given)
-    other_down = traded(given_down)
+    down_weight = down_weight.transpose(0, 2, 1)
+    tiles, keep, give = first_tiles(n, turned, pre_gain, post_gain, gate_weight, up_weight, down_weight)
+    tiles, low = lax.optimization_barrier((tiles, low))
+    other = traded(give)
     got = exchange(tiles, RA)
     got = jnp.sum(got.astype(f32), axis=0)
     squares = total(got[2 * size : 2 * size + 2])
@@ -226,10 +233,10 @@
         return to_all(hidden, axes).reshape(-1, ntok)
 
     hidden = hidden_of(got[: 2 * size] * scale_in, RA)
-    parts = decoded(to_all(coded(project(down_weight[0], hidden)), SUM))
+    parts = decoded(to_all(coded(down_project(down_weight[0], hidden)), SUM))
     branch = jnp.concatenate(pair(*jnp.sum(parts.reshape(2, -1, width, ntok), axis=1)))
 
-    tiles, gained, last = second_tiles(n // 2, branch, side, other, weights)
+    tiles, start, gained, last = second_tiles(n // 2, held, branch, keep, other)
     got = jnp.sum(exchange(tiles, PART).astype(f32), axis=0)
     sums = got[4 * size : 4 * size + 3] + got[4 * size + 3 : 4 * size + 6]
     branch_sq, gained_sq, cross = sums[0:1], sums[1:2], sums[2:3]
@@ -240,7 +247,8 @@
 
     both = (RESIDUAL * got[2 * size : 4 * size] + scale_out * got[: 2 * size]) * scale_in
     hidden = hidden_of(both, PART)
-    halves = pair(coded(project(down, hidden)), coded(project(other_down, hidden)))
+    step = -(-held // 128) * 128
+    halves = pair(*[coded(down_project(x[:, 2 * step : 2 * step + held], hidden)) for x in (keep, other)])
     members = lax.axis_size("cb")
     parts = jnp.concatenate([jnp.broadcast_to(half[None], (members, *half.shape)) for half in halves])
     branch = jnp.sum(decoded(exchange(parts, SUM)), axis=0)

time: 126 us -> 122 us (0.968)
  blocking collectives: 84.5 us -> 97.9 us
  waiting for transfers between devices: 16.1 us -> 7.64 us
  starting transfers between devices: 13.4 us -> 8.94 us
  other arithmetic: 4.05 us -> 1.32 us
  local copies, waits for them, and re-layouts: 3.32 us -> 1.84 us
    all_to_all x5 -> x6, blocking collectives: 84.5 us -> 97.9 us  [exchange(): return lax.all_to_all(tiles, axis, 0, 0, tiled=True)]
    all_to_all x2 -> x1, waiting for transfers between devices: 15.5 us -> 6.02 us  [exchange(): return lax.all_to_all(tiles, axis, 0, 0, tiled=True)]
    all_to_all x2 -> x1, starting transfers between devices: 11.7 us -> 7.49 us  [exchange(): return lax.all_to_all(tiles, axis, 0, 0, tiled=True)]
    select_n x4 -> x2, other arithmetic: 1.97 us -> 0.03 us  [pair(): return (jnp.where(low, first, second), jnp.where(low, second, first))]
  transfers between devices with their start and end apart: 4 -> 2, of which waited for: 3 -> 2; matrix products, arithmetic and copies ran while one was open for 0% -> 0% of each run, Pallas kernels for 0% -> 0%
where the time goes in v1:
time: 122 us
  blocking collectives  97.9 us (80%)
  starting transfers between devices  8.94 us (7%)
  waiting for transfers between devices  7.64 us (6%)
  Pallas kernels  3.33 us (3%)
  local copies, waits for them, and re-layouts  1.84 us (2%)
  other arithmetic  1.32 us (1%)
    all_to_all x6, blocking collectives, exchange(): return lax.all_to_all(tiles, axis, 0, 0, tiled=True)  97.9 us
    all_to_all x1, starting transfers between devices, exchange(): return lax.all_to_all(tiles, axis, 0, 0, tiled=True)  7.49 us
    all_to_all x1, waiting for transfers between devices, exchange(): return lax.all_to_all(tiles, axis, 0, 0, tiled=True)  6.02 us
    pallas_call x1, Pallas kernels, first_tiles(): pl.pallas_call(first_kernel, out_shape=outs, in_specs=[hbm] * 6, out_spec...  2.71 us
  transfers between devices with their start and end apart: 2, of which 2 were waited for; matrix products, arithmetic and copies ran while one was open for 0% of the time, Pallas kernels for 0%

profile of v1, /device:TPU:1, one launch (start us, length us, event | category | flops | bytes accessed | tf_op | source)
XLA Modules:
  0.0 121.7 jit_solution(13675109535153401985)
XLA Ops:
  0.0 2.7 %shard_map.64 = (bf16[32,48,128]{2,1,0:T(8,128)(2,1)}, bf16[64,1408]{1,0:T(8,128)(2,1)}, bf16[64,1408]{1,0:T(8,128)(2,1)}) custom-call(bf16[64,128]{1,0:T(8,128)(2,1)} %bitcast.40, f32[2,64]{1,0:T(2,128)} %refs_1_.1, f32[2,64]{1,0:T(2,128)} %refs_2_.1, bf16[2,64,704]{2,1,0:T(8,128)(2,1)} %refs_3_.1, bf16[2,64,704]{2,1,0:T(8,128)(2,1)} %refs_4_.1, ...), custom_call_target="tpu_custom_call" | custom-call | tf_op jit(solution)/shard_map/pallas_call | solution.py:151
  2.7 25.9 %all_to_all.35 = bf16[32,48,128]{2,1,0:T(8,128)(2,1)S(1)} all-to-all(bf16[32,48,128]{2,1,0:T(8,128)(2,1)} %get-tuple-element.16), channel_id=1, replica_groups=mesh['z'=8,'y_high'=2,'y_low'=2,'cb'=8] {'z','y_high','y_low'}, dimensions={0} | all-to-all | bytes 786432 | tf_op jit(solution)/shard_map/all_to_all | solution.py:21
  28.6 0.1 convert_reduce_fusion.1
  28.7 14.8 %all_to_all.36 = bf16[32,22,128]{2,1,0:T(8,128)(2,1)S(1)} all-to-all(bf16[32,22,128]{2,1,0:T(8,128)(2,1)S(1)} %broadcast_in_dim.18), channel_id=1, replica_groups=mesh['z'=8,'y_high'=2,'y_low'=2,'cb'=8] {'z','y_high','y_low'}, dimensions={0} | all-to-all | bytes 360448 | tf_op jit(solution)/shard_map/all_to_all | solution.py:21
  43.5 0.0 copy-start.1
  43.5 0.1 reshape.191
  43.6 0.9 copy-done.1
  44.4 0.2 abs_reduce_fusion.2
  44.7 0.7 broadcast_in_dim.20
  45.4 0.0 copy-start.2
  45.4 7.5 %all-to-all-start.2 = ((f16[16,72,128]{2,1,0:T(8,128)(2,1)}), f16[16,72,128]{2,1,0:T(8,128)(2,1)S(1)}, u32[]{:S(2)}, u32[]{:S(2)}) async-start(f16[16,72,128]{2,1,0:T(8,128)(2,1)} %broadcast_in_dim.20), calls=%async_computation.2 | async-start | bytes 589824 | tf_op jit(solution)/shard_map/all_to_all | solution.py:21
  52.9 0.0 copy-done.2
  52.9 1.4 %collective-permute-start = (bf16[64,1408]{1,0:T(8,128)(2,1)S(1)}, bf16[64,1408]{1,0:T(8,128)(2,1)S(1)}, u32[]{:S(2)}, u32[]{:S(2)}) collective-permute-start(bf16[64,1408]{1,0:T(8,128)(2,1)S(1)} %copy-done.2), channel_id=1, source_target_pairs={{0,8},{8,0},{1,9},{9,1},{2,10},{10,2},{3,11},{11,3},{4,12},{12,4},... | collective-permute-start | bytes 540680 | tf_op jit(solution)/shard_map/ppermute | solution.py:208
  54.4 6.0 %all-to-all-done.2 = f16[16,72,128]{2,1,0:T(8,128)(2,1)S(1)} async-done(((f16[16,72,128]{2,1,0:T(8,128)(2,1)}), f16[16,72,128]{2,1,0:T(8,128)(2,1)S(1)}, u32[]{:S(2)}, u32[]{:S(2)}) %all-to-all-start.2) | async-done | bytes 294944 | tf_op jit(solution)/shard_map/all_to_all | solution.py:21
  60.5 0.0 copy-start
  60.5 1.6 %collective-permute-done.refs_2_ = bf16[64,1408]{1,0:T(8,128)(2,1)S(1)} collective-permute-done((bf16[64,1408]{1,0:T(8,128)(2,1)S(1)}, bf16[64,1408]{1,0:T(8,128)(2,1)S(1)}, u32[]{:S(2)}, u32[]{:S(2)}) %collective-permute-start) | collective-permute-done | bytes 180256 | tf_op jit(solution)/shard_map/ppermute | solution.py:208
  62.2 0.0 copy-done
  62.2 0.6 shard_map.65
  62.8 17.9 %all_to_all.37 = bf16[16,96,128]{2,1,0:T(8,128)(2,1)S(1)} all-to-all(bf16[16,96,128]{2,1,0:T(8,128)(2,1)S(1)} %get-tuple-element.21), channel_id=1, replica_groups=mesh['z'=8,'y_high'=2,'y_low'=2,'cb'=8] {'z','y_high'}, dimensions={0} | all-to-all | bytes 786432 | tf_op jit(solution)/shard_map/all_to_all | solution.py:21
  80.7 0.1 convert_reduce_fusion
  80.8 13.7 %all_to_all.38 = bf16[16,22,128]{2,1,0:T(8,128)(2,1)S(1)} all-to-all(bf16[16,22,128]{2,1,0:T(8,128)(2,1)S(1)} %broadcast_in_dim.21), channel_id=1, replica_groups=mesh['z'=8,'y_high'=2,'y_low'=2,'cb'=8] {'z','y_high'}, dimensions={0} | all-to-all | bytes 180224 | tf_op jit(solution)/shard_map/all_to_all | solution.py:21
  94.5 0.2 abs_reduce_fusion.1
  94.7 0.2 abs_reduce_fusion
  95.1 0.1 pad_maximum_fusion
  95.1 14.2 %all_to_all.39 = f16[16,72,128]{2,1,0:T(8,128)(2,1)S(1)} all-to-all(f16[16,72,128]{2,1,0:T(8,128)(2,1)S(1)} %pad_maximum_fusion), channel_id=1, replica_groups=mesh['z'=8,'y_high'=2,'y_low'=2,'cb'=8] {'y_low','cb'}, dimensions={0} | all-to-all | bytes 589824 | tf_op jit(solution)/shard_map/all_to_all | solution.py:21
  109.4 0.1 fusion
  109.5 11.6 %all_to_all.40 = f32[32,1,128]{2,1,0:T(1,128)S(1)} all-to-all(f32[32,1,128]{2,1,0:T(1,128)S(1)} %broadcast_in_dim.26), channel_id=1, replica_groups=mesh['z'=8,'y_high'=2,'y_low'=2,'cb'=8] {'z','y_high','y_low'}, dimensions={0} | all-to-all | bytes 32768 | tf_op jit(solution)/shard_map/all_to_all | solution.py:21
  121.1 0.6 fusion.9
  (34 shorter events, 0.6 us)
Async XLA Ops:
  43.5 0.9 copy-start.1
  45.4 7.5 %copy-start.2 = (bf16[64,1408]{1,0:T(8,128)(2,1)S(1)}, bf16[64,1408]{1,0:T(8,128)(2,1)}, u32[]{:S(2)}) copy-start(bf16[64,1408]{1,0:T(8,128)(2,1)} %get-tuple-element.18) | copy-start | bytes 540676
  45.4 15.0 %all-to-all-start.2 = ((f16[16,72,128]{2,1,0:T(8,128)(2,1)}), f16[16,72,128]{2,1,0:T(8,128)(2,1)S(1)}, u32[]{:S(2)}, u32[]{:S(2)}) async-start(f16[16,72,128]{2,1,0:T(8,128)(2,1)} %broadcast_in_dim.20), calls=%async_computation.2 | async-start | bytes 589824 | tf_op jit(solution)/shard_map/all_to_all | solution.py:21
  52.9 9.2 %collective-permute-start = (bf16[64,1408]{1,0:T(8,128)(2,1)S(1)}, bf16[64,1408]{1,0:T(8,128)(2,1)S(1)}, u32[]{:S(2)}, u32[]{:S(2)}) collective-permute-start(bf16[64,1408]{1,0:T(8,128)(2,1)S(1)} %copy-done.2), channel_id=1, source_target_pairs={{0,8},{8,0},{1,9},{9,1},{2,10},{10,2},{3,11},{11,3},{4,12},{12,4},... | collective-permute-start | bytes 540680 | tf_op jit(solution)/shard_map/ppermute | solution.py:208
  60.5 1.7 %copy-start = (bf16[64,1408]{1,0:T(8,128)(2,1)S(1)}, bf16[64,1408]{1,0:T(8,128)(2,1)}, u32[]{:S(2)}) copy-start(bf16[64,1408]{1,0:T(8,128)(2,1)} %get-tuple-element.17.refs_1_) | copy-start | bytes 540676

commit v2 on v1

--- a/solution.py
+++ b/solution.py
@@ -167,10 +167,10 @@
 
 
 def second_kernel(*refs):
-    branch_ref, mine_ref, other_ref, out_ref, start_ref, gained_ref, last_ref, flat_ref, stage_ref = refs
+    branch_ref, mine_ref, side_ref, other_ref, out_ref, start_ref, gained_ref, last_ref, flat_ref, stage_ref = refs
     width, ntok = gained_ref.shape
-    held, step = flat_ref.shape[1], (mine_ref.shape[1] - ntok - 128) // 3
-    sides = [ref[:, 3 * step :] for ref in (mine_ref, other_ref)]
+    held, step = flat_ref.shape[1], mine_ref.shape[1] // 3
+    sides = side_ref[...], other_ref[:, 3 * step :]
     start = jnp.concatenate([side[:, :ntok] for side in sides]).astype(f32)
     start_ref[...] = start[:width]
     gains = [jnp.concatenate([gain_of(side[:, ntok:], i) for side in sides]) for i in range(3)]
@@ -221,9 +221,12 @@
     held = gate_weight.shape[2] // 2
     down_weight = down_weight.transpose(0, 2, 1)
     tiles, keep, give = first_tiles(n, turned, pre_gain, post_gain, gate_weight, up_weight, down_weight)
-    tiles, low = lax.optimization_barrier((tiles, low))
+    down_now = jnp.where(low, down_weight[0], down_weight[0] * 1)
+    tiles, low, down_now = lax.optimization_barrier((tiles, low, down_now))
     other = traded(give)
     got = exchange(tiles, RA)
+    step = -(-held // 128) * 128
+    got, keep, side = lax.optimization_barrier((got, keep[:, : 3 * step], keep[:, 3 * step :]))
     got = jnp.sum(got.astype(f32), axis=0)
     squares = total(got[2 * size : 2 * size + 2])
     scale_in = lax.rsqrt(squares / D + EPSILON)
@@ -233,10 +236,10 @@
         return to_all(hidden, axes).reshape(-1, ntok)
 
     hidden = hidden_of(got[: 2 * size] * scale_in, RA)
-    parts = decoded(to_all(coded(down_project(down_weight[0], hidden)), SUM))
+    parts = decoded(to_all(coded(down_project(down_now, hidden)), SUM))
     branch = jnp.concatenate(pair(*jnp.sum(parts.reshape(2, -1, width, ntok), axis=1)))
 
-    tiles, start, gained, last = second_tiles(n // 2, held, branch, keep, other)
+    tiles, start, gained, last = second_tiles(n // 2, held, branch, keep, side, other)
     got = jnp.sum(exchange(tiles, PART).astype(f32), axis=0)
     sums = got[4 * size : 4 * size + 3] + got[4 * size + 3 : 4 * size + 6]
     branch_sq, gained_sq, cross = sums[0:1], sums[1:2], sums[2:3]
@@ -247,7 +250,6 @@
 
     both = (RESIDUAL * got[2 * size : 4 * size] + scale_out * got[: 2 * size]) * scale_in
     hidden = hidden_of(both, PART)
-    step = -(-held // 128) * 128
     halves = pair(*[coded(down_project(x[:, 2 * step : 2 * step + held], hidden)) for x in (keep, other)])
     members = lax.axis_size("cb")
     parts = jnp.concatenate([jnp.broadcast_to(half[None], (members, *half.shape)) for half in halves])

time: 122 us -> 122 us (level)
  blocking collectives: 97.9 us -> 72.1 us
  waiting for transfers between devices: 7.64 us -> 21.4 us
  starting transfers between devices: 8.94 us -> 21.1 us
    all_to_all x6 -> x5, blocking collectives: 97.9 us -> 72.1 us  [exchange(): return lax.all_to_all(tiles, axis, 0, 0, tiled=True)]
    all_to_all x1 -> x2, waiting for transfers between devices: 6.02 us -> 19.8 us  [exchange(): return lax.all_to_all(tiles, axis, 0, 0, tiled=True)]
    all_to_all x1 -> x2, starting transfers between devices: 7.49 us -> 19.7 us  [exchange(): return lax.all_to_all(tiles, axis, 0, 0, tiled=True)]
  transfers between devices with their start and end apart: 2 -> 3, of which waited for: 2 -> 3; matrix products, arithmetic and copies ran while one was open for 0% -> 0% of each run, Pallas kernels for 0% -> 0%
where the time goes in v2:
time: 122 us
  blocking collectives  72.1 us (59%)
  waiting for transfers between devices  21.4 us (18%)
  starting transfers between devices  21.1 us (17%)
  Pallas kernels  3.32 us (3%)
  local copies, waits for them, and re-layouts  1.89 us (2%)
  other arithmetic  1.31 us (1%)
    all_to_all x5, blocking collectives, exchange(): return lax.all_to_all(tiles, axis, 0, 0, tiled=True)  72.1 us
    all_to_all x2, waiting for transfers between devices, exchange(): return lax.all_to_all(tiles, axis, 0, 0, tiled=True)  19.8 us
    all_to_all x2, starting transfers between devices, exchange(): return lax.all_to_all(tiles, axis, 0, 0, tiled=True)  19.7 us
    pallas_call x1, Pallas kernels, first_tiles(): pl.pallas_call(first_kernel, out_shape=outs, in_specs=[hbm] * 6, out_spec...  2.7 us
  transfers between devices with their start and end apart: 3, of which 3 were waited for; matrix products, arithmetic and copies ran while one was open for 0% of the time, Pallas kernels for 0%

profile of v2, /device:TPU:1, one launch (start us, length us, event | category | flops | bytes accessed | tf_op | source)
XLA Modules:
  0.0 121.9 jit_solution(6523616212917969575)
XLA Ops:
  0.0 0.9 slice_bitcast_fusion
  0.9 2.7 %shard_map.64 = (bf16[32,48,128]{2,1,0:T(8,128)(2,1)}, bf16[64,1408]{1,0:T(8,128)(2,1)}, bf16[64,1408]{1,0:T(8,128)(2,1)}) custom-call(bf16[64,128]{1,0:T(8,128)(2,1)} %bitcast.36, f32[2,64]{1,0:T(2,128)} %refs_1_.1, f32[2,64]{1,0:T(2,128)} %refs_2_.1, bf16[2,64,704]{2,1,0:T(8,128)(2,1)} %refs_3_.1, bf16[2,64,704]{2,1,0:T(8,128)(2,1)} %refs_4_.1, ...), custom_call_target="tpu_custom_call" | custom-call | tf_op jit(solution)/shard_map/pallas_call | solution.py:151
  3.6 0.0 copy-start
  3.6 12.2 %all-to-all-start = ((bf16[32,48,128]{2,1,0:T(8,128)(2,1)}), bf16[32,48,128]{2,1,0:T(8,128)(2,1)S(1)}, u32[]{:S(2)}, u32[]{:S(2)}) async-start(bf16[32,48,128]{2,1,0:T(8,128)(2,1)} %get-tuple-element.21), calls=%async_computation | async-start | bytes 786432 | tf_op jit(solution)/shard_map/all_to_all | solution.py:21
  15.8 0.0 copy-done
  15.8 13.8 %all-to-all-done = bf16[32,48,128]{2,1,0:T(8,128)(2,1)S(1)} async-done(((bf16[32,48,128]{2,1,0:T(8,128)(2,1)}), bf16[32,48,128]{2,1,0:T(8,128)(2,1)S(1)}, u32[]{:S(2)}, u32[]{:S(2)}) %all-to-all-start) | async-done | bytes 393248 | tf_op jit(solution)/shard_map/all_to_all | solution.py:21
  29.6 0.1 convert_reduce_fusion.1
  29.8 14.8 %all_to_all.35 = bf16[32,22,128]{2,1,0:T(8,128)(2,1)S(1)} all-to-all(bf16[32,22,128]{2,1,0:T(8,128)(2,1)S(1)} %broadcast_in_dim.18), channel_id=1, replica_groups=mesh['z'=8,'y_high'=2,'y_low'=2,'cb'=8] {'z','y_high','y_low'}, dimensions={0} | all-to-all | bytes 360448 | tf_op jit(solution)/shard_map/all_to_all | solution.py:21
  44.5 0.1 reshape.191
  44.6 0.2 abs_reduce_fusion.2
  44.9 0.7 broadcast_in_dim.20
  45.6 0.0 copy-start.1
  45.6 7.5 %all-to-all-start.2 = ((f16[16,72,128]{2,1,0:T(8,128)(2,1)}), f16[16,72,128]{2,1,0:T(8,128)(2,1)S(1)}, u32[]{:S(2)}, u32[]{:S(2)}) async-start(f16[16,72,128]{2,1,0:T(8,128)(2,1)} %broadcast_in_dim.20), calls=%async_computation.2 | async-start | bytes 589824 | tf_op jit(solution)/shard_map/all_to_all | solution.py:21
  53.1 0.0 copy-done.1
  53.1 1.4 %collective-permute-start = (bf16[64,1408]{1,0:T(8,128)(2,1)S(1)}, bf16[64,1408]{1,0:T(8,128)(2,1)S(1)}, u32[]{:S(2)}, u32[]{:S(2)}) collective-permute-start(bf16[64,1408]{1,0:T(8,128)(2,1)S(1)} %copy-done.1), channel_id=1, source_target_pairs={{0,8},{8,0},{1,9},{9,1},{2,10},{10,2},{3,11},{11,3},{4,12},{12,4},... | collective-permute-start | bytes 540680 | tf_op jit(solution)/shard_map/ppermute | solution.py:208
  54.6 6.0 %all-to-all-done.2 = f16[16,72,128]{2,1,0:T(8,128)(2,1)S(1)} async-done(((f16[16,72,128]{2,1,0:T(8,128)(2,1)}), f16[16,72,128]{2,1,0:T(8,128)(2,1)S(1)}, u32[]{:S(2)}, u32[]{:S(2)}) %all-to-all-start.2) | async-done | bytes 294944 | tf_op jit(solution)/shard_map/all_to_all | solution.py:21
  60.7 1.6 %collective-permute-done.refs_3_ = bf16[64,1408]{1,0:T(8,128)(2,1)S(1)} collective-permute-done((bf16[64,1408]{1,0:T(8,128)(2,1)S(1)}, bf16[64,1408]{1,0:T(8,128)(2,1)S(1)}, u32[]{:S(2)}, u32[]{:S(2)}) %collective-permute-start) | collective-permute-done | bytes 180256 | tf_op jit(solution)/shard_map/ppermute | solution.py:208
  62.4 0.6 shard_map.65
  63.0 17.9 %all_to_all.36 = bf16[16,96,128]{2,1,0:T(8,128)(2,1)S(1)} all-to-all(bf16[16,96,128]{2,1,0:T(8,128)(2,1)S(1)} %get-tuple-element.29), channel_id=1, replica_groups=mesh['z'=8,'y_high'=2,'y_low'=2,'cb'=8] {'z','y_high'}, dimensions={0} | all-to-all | bytes 786432 | tf_op jit(solution)/shard_map/all_to_all | solution.py:21
  80.8 0.1 convert_reduce_fusion
  81.0 13.7 %all_to_all.37 = bf16[16,22,128]{2,1,0:T(8,128)(2,1)S(1)} all-to-all(bf16[16,22,128]{2,1,0:T(8,128)(2,1)S(1)} %broadcast_in_dim.21), channel_id=1, replica_groups=mesh['z'=8,'y_high'=2,'y_low'=2,'cb'=8] {'z','y_high'}, dimensions={0} | all-to-all | bytes 180224 | tf_op jit(solution)/shard_map/all_to_all | solution.py:21
  94.7 0.2 abs_reduce_fusion.1
  94.9 0.2 abs_reduce_fusion
  95.2 0.1 pad_maximum_fusion
  95.3 14.2 %all_to_all.38 = f16[16,72,128]{2,1,0:T(8,128)(2,1)S(1)} all-to-all(f16[16,72,128]{2,1,0:T(8,128)(2,1)S(1)} %pad_maximum_fusion), channel_id=1, replica_groups=mesh['z'=8,'y_high'=2,'y_low'=2,'cb'=8] {'y_low','cb'}, dimensions={0} | all-to-all | bytes 589824 | tf_op jit(solution)/shard_map/all_to_all | solution.py:21
  109.7 11.6 %all_to_all.39 = f32[32,1,128]{2,1,0:T(1,128)S(1)} all-to-all(f32[32,1,128]{2,1,0:T(1,128)S(1)} %broadcast_in_dim.26), channel_id=1, replica_groups=mesh['z'=8,'y_high'=2,'y_low'=2,'cb'=8] {'z','y_high','y_low'}, dimensions={0} | all-to-all | bytes 32768 | tf_op jit(solution)/shard_map/all_to_all | solution.py:21
  121.3 0.6 fusion.7
  (37 shorter events, 0.7 us)
Async XLA Ops:
  3.6 12.2 %copy-start = (bf16[64,1408]{1,0:T(8,128)(2,1)S(1)}, bf16[64,1408]{1,0:T(8,128)(2,1)}, u32[]{:S(2)}) copy-start(bf16[64,1408]{1,0:T(8,128)(2,1)} %get-tuple-element.22) | copy-start | bytes 540676
  3.6 26.0 %all-to-all-start = ((bf16[32,48,128]{2,1,0:T(8,128)(2,1)}), bf16[32,48,128]{2,1,0:T(8,128)(2,1)S(1)}, u32[]{:S(2)}, u32[]{:S(2)}) async-start(bf16[32,48,128]{2,1,0:T(8,128)(2,1)} %get-tuple-element.21), calls=%async_computation | async-start | bytes 786432 | tf_op jit(solution)/shard_map/all_to_all | solution.py:21
  45.6 7.5 %copy-start.1 = (bf16[64,1408]{1,0:T(8,128)(2,1)S(1)}, bf16[64,1408]{1,0:T(8,128)(2,1)}, u32[]{:S(2)}) copy-start(bf16[64,1408]{1,0:T(8,128)(2,1)} %get-tuple-element.26) | copy-start | bytes 540676
  45.6 15.0 %all-to-all-start.2 = ((f16[16,72,128]{2,1,0:T(8,128)(2,1)}), f16[16,72,128]{2,1,0:T(8,128)(2,1)S(1)}, u32[]{:S(2)}, u32[]{:S(2)}) async-start(f16[16,72,128]{2,1,0:T(8,128)(2,1)} %broadcast_in_dim.20), calls=%async_computation.2 | async-start | bytes 589824 | tf_op jit(solution)/shard_map/all_to_all | solution.py:21
  53.1 9.2 %collective-permute-start = (bf16[64,1408]{1,0:T(8,128)(2,1)S(1)}, bf16[64,1408]{1,0:T(8,128)(2,1)S(1)}, u32[]{:S(2)}, u32[]{:S(2)}) collective-permute-start(bf16[64,1408]{1,0:T(8,128)(2,1)S(1)} %copy-done.1), channel_id=1, source_target_pairs={{0,8},{8,0},{1,9},{9,1},{2,10},{10,2},{3,11},{11,3},{4,12},{12,4},... | collective-permute-start | bytes 540680 | tf_op jit(solution)/shard_map/ppermute | solution.py:208

commit v3 on v2

--- a/solution.py
+++ b/solution.py
@@ -13,17 +13,17 @@
 f32 = jnp.float32
 bf16 = jnp.bfloat16
 RA = ("z", "y_high", "y_low")
-PART = ("z", "y_high")
+PARTS = [[4 * z + y for z in range(8) for y in ys] for ys in ((0, 3), (1, 2))]
 SUM = ("y_low", "cb")
 
 
-def exchange(tiles, axis):
-    return lax.all_to_all(tiles, axis, 0, 0, tiled=True)
-
-
-def to_all(tile, axis):
-    n = lax.axis_size(axis)
-    return exchange(jnp.broadcast_to(tile[None], (n, *tile.shape)), axis)
+def exchange(tiles, axis, groups=None):
+    return lax.all_to_all(tiles, axis, 0, 0, axis_index_groups=groups, tiled=True)
+
+
+def to_all(tile, axis, groups=None):
+    n = len(groups[0]) if groups else lax.axis_size(axis)
+    return exchange(jnp.broadcast_to(tile[None], (n, *tile.shape)), axis, groups)
 
 
 def coded(part):
@@ -122,7 +122,7 @@
         writes.append(pltpu.make_async_copy(tiles_ref.at[part], out_ref.at[part], out_sems.at[g]))
         writes[-1].start()
 
-    low = lax.axis_index("y_low") == 0
+    low = lax.axis_index("y_low") == lax.axis_index("y_high")
     width, wide = traded_refs[0].shape[1], turn_ref.shape[1]
     half, step = width // 2, wide // 2
     for k, ref in enumerate(traded_refs):
@@ -231,16 +231,16 @@
     squares = total(got[2 * size : 2 * size + 2])
     scale_in = lax.rsqrt(squares / D + EPSILON)
 
-    def hidden_of(both, axes):
+    def hidden_of(both, groups):
         hidden = (jax.nn.silu(both[:size]) * both[size:]).astype(bf16)
-        return to_all(hidden, axes).reshape(-1, ntok)
-
-    hidden = hidden_of(got[: 2 * size] * scale_in, RA)
+        return to_all(hidden, RA, groups).reshape(-1, ntok)
+
+    hidden = hidden_of(got[: 2 * size] * scale_in, None)
     parts = decoded(to_all(coded(down_project(down_now, hidden)), SUM))
     branch = jnp.concatenate(pair(*jnp.sum(parts.reshape(2, -1, width, ntok), axis=1)))
 
     tiles, start, gained, last = second_tiles(n // 2, held, branch, keep, side, other)
-    got = jnp.sum(exchange(tiles, PART).astype(f32), axis=0)
+    got = jnp.sum(exchange(tiles, RA, PARTS).astype(f32), axis=0)
     sums = got[4 * size : 4 * size + 3] + got[4 * size + 3 : 4 * size + 6]
     branch_sq, gained_sq, cross = sums[0:1], sums[1:2], sums[2:3]
     scale_out = lax.rsqrt(branch_sq / D + EPSILON)
@@ -249,7 +249,7 @@
     stream = RESIDUAL * start + gained * scale_out
 
     both = (RESIDUAL * got[2 * size : 4 * size] + scale_out * got[: 2 * size]) * scale_in
-    hidden = hidden_of(both, PART)
+    hidden = hidden_of(both, PARTS)
     halves = pair(*[coded(down_project(x[:, 2 * step : 2 * step + held], hidden)) for x in (keep, other)])
     members = lax.axis_size("cb")
     parts = jnp.concatenate([jnp.broadcast_to(half[None], (members, *half.shape)) for half in halves])

time: 122 us -> 122 us (level)
  no operation moved by 1% of the time
where the time goes in v3:
time: 122 us; the launch traced here: 121 us
  blocking collectives  71.3 us (58%)
  waiting for transfers between devices  21.4 us (18%)
  starting transfers between devices  21.1 us (17%)
  Pallas kernels  3.32 us (3%)
  local copies, waits for them, and re-layouts  1.89 us (2%)
  other arithmetic  1.31 us (1%)
    all_to_all x5, blocking collectives, exchange(): lax.all_to_all(tiles, axis, 0, 0, axis_index_groups=groups, tiled=True)  71.3 us
    all_to_all x2, waiting for transfers between devices, exchange(): lax.all_to_all(tiles, axis, 0, 0, axis_index_groups=groups, tiled=True)  19.8 us
    all_to_all x2, starting transfers between devices, exchange(): lax.all_to_all(tiles, axis, 0, 0, axis_index_groups=groups, tiled=True)  19.7 us
    pallas_call x1, Pallas kernels, first_tiles(): pl.pallas_call(first_kernel, out_shape=outs, in_specs=[hbm] * 6, out_spec...  2.7 us
  transfers between devices with their start and end apart: 3, of which 3 were waited for; matrix products, arithmetic and copies ran while one was open for 0% of the time, Pallas kernels for 0%

profile of v3, /device:TPU:1, one launch (start us, length us, event | category | flops | bytes accessed | tf_op | source)
XLA Modules:
  0.0 121.2 jit_solution(16564060294084777839)
XLA Ops:
  0.0 0.9 slice_bitcast_fusion
  0.9 2.7 %shard_map.64 = (bf16[32,48,128]{2,1,0:T(8,128)(2,1)}, bf16[64,1408]{1,0:T(8,128)(2,1)}, bf16[64,1408]{1,0:T(8,128)(2,1)}) custom-call(bf16[64,128]{1,0:T(8,128)(2,1)} %bitcast.36, f32[2,64]{1,0:T(2,128)} %refs_1_.1, f32[2,64]{1,0:T(2,128)} %refs_2_.1, bf16[2,64,704]{2,1,0:T(8,128)(2,1)} %refs_3_.1, bf16[2,64,704]{2,1,0:T(8,128)(2,1)} %refs_4_.1, ...), custom_call_target="tpu_custom_call" | custom-call | tf_op jit(solution)/shard_map/pallas_call | solution.py:151
  3.6 0.0 copy-start
  3.6 12.2 %all-to-all-start = ((bf16[32,48,128]{2,1,0:T(8,128)(2,1)}), bf16[32,48,128]{2,1,0:T(8,128)(2,1)S(1)}, u32[]{:S(2)}, u32[]{:S(2)}) async-start(bf16[32,48,128]{2,1,0:T(8,128)(2,1)} %get-tuple-element.21), calls=%async_computation | async-start | bytes 786432 | tf_op jit(solution)/shard_map/all_to_all | solution.py:21
  15.8 0.0 copy-done
  15.8 13.8 %all-to-all-done = bf16[32,48,128]{2,1,0:T(8,128)(2,1)S(1)} async-done(((bf16[32,48,128]{2,1,0:T(8,128)(2,1)}), bf16[32,48,128]{2,1,0:T(8,128)(2,1)S(1)}, u32[]{:S(2)}, u32[]{:S(2)}) %all-to-all-start) | async-done | bytes 393248 | tf_op jit(solution)/shard_map/all_to_all | solution.py:21
  29.6 0.1 convert_reduce_fusion.1
  29.8 14.8 %all_to_all.35 = bf16[32,22,128]{2,1,0:T(8,128)(2,1)S(1)} all-to-all(bf16[32,22,128]{2,1,0:T(8,128)(2,1)S(1)} %broadcast_in_dim.18), channel_id=1, replica_groups=mesh['z'=8,'y_high'=2,'y_low'=2,'cb'=8] {'z','y_high','y_low'}, dimensions={0} | all-to-all | bytes 360448 | tf_op jit(solution)/shard_map/all_to_all | solution.py:21
  44.5 0.1 reshape.191
  44.6 0.2 abs_reduce_fusion.2
  44.9 0.7 broadcast_in_dim.20
  45.6 0.0 copy-start.1
  45.6 7.5 %all-to-all-start.2 = ((f16[16,72,128]{2,1,0:T(8,128)(2,1)}), f16[16,72,128]{2,1,0:T(8,128)(2,1)S(1)}, u32[]{:S(2)}, u32[]{:S(2)}) async-start(f16[16,72,128]{2,1,0:T(8,128)(2,1)} %broadcast_in_dim.20), calls=%async_computation.2 | async-start | bytes 589824 | tf_op jit(solution)/shard_map/all_to_all | solution.py:21
  53.1 0.0 copy-done.1
  53.1 1.4 %collective-permute-start = (bf16[64,1408]{1,0:T(8,128)(2,1)S(1)}, bf16[64,1408]{1,0:T(8,128)(2,1)S(1)}, u32[]{:S(2)}, u32[]{:S(2)}) collective-permute-start(bf16[64,1408]{1,0:T(8,128)(2,1)S(1)} %copy-done.1), channel_id=1, source_target_pairs={{0,8},{8,0},{1,9},{9,1},{2,10},{10,2},{3,11},{11,3},{4,12},{12,4},... | collective-permute-start | bytes 540680 | tf_op jit(solution)/shard_map/ppermute | solution.py:208
  54.6 6.0 %all-to-all-done.2 = f16[16,72,128]{2,1,0:T(8,128)(2,1)S(1)} async-done(((f16[16,72,128]{2,1,0:T(8,128)(2,1)}), f16[16,72,128]{2,1,0:T(8,128)(2,1)S(1)}, u32[]{:S(2)}, u32[]{:S(2)}) %all-to-all-start.2) | async-done | bytes 294944 | tf_op jit(solution)/shard_map/all_to_all | solution.py:21
  60.7 1.6 %collective-permute-done.refs_3_ = bf16[64,1408]{1,0:T(8,128)(2,1)S(1)} collective-permute-done((bf16[64,1408]{1,0:T(8,128)(2,1)S(1)}, bf16[64,1408]{1,0:T(8,128)(2,1)S(1)}, u32[]{:S(2)}, u32[]{:S(2)}) %collective-permute-start) | collective-permute-done | bytes 180256 | tf_op jit(solution)/shard_map/ppermute | solution.py:208
  62.4 0.6 shard_map.65
  63.0 16.8 %all_to_all.36 = bf16[16,96,128]{2,1,0:T(8,128)(2,1)S(1)} all-to-all(bf16[16,96,128]{2,1,0:T(8,128)(2,1)S(1)} %get-tuple-element.29), channel_id=1, replica_groups={{0,24,32,56,64,88,96,120,128,152,160,184,192,216,224,248},{8,16,40,48,7..., dimensions={0} | all-to-all | bytes 786432 | tf_op jit(solution)/shard_map/all_to_all | solution.py:21
  79.8 0.1 convert_reduce_fusion
  80.0 13.4 %all_to_all.37 = bf16[16,22,128]{2,1,0:T(8,128)(2,1)S(1)} all-to-all(bf16[16,22,128]{2,1,0:T(8,128)(2,1)S(1)} %broadcast_in_dim.21), channel_id=1, replica_groups={{0,24,32,56,64,88,96,120,128,152,160,184,192,216,224,248},{8,16,40,48,7..., dimensions={0} | all-to-all | bytes 180224 | tf_op jit(solution)/shard_map/all_to_all | solution.py:21
  93.4 0.2 abs_reduce_fusion.1
  93.6 0.2 abs_reduce_fusion
  93.9 0.1 pad_maximum_fusion
  94.0 14.7 %all_to_all.38 = f16[16,72,128]{2,1,0:T(8,128)(2,1)S(1)} all-to-all(f16[16,72,128]{2,1,0:T(8,128)(2,1)S(1)} %pad_maximum_fusion), channel_id=1, replica_groups=mesh['z'=8,'y_high'=2,'y_low'=2,'cb'=8] {'y_low','cb'}, dimensions={0} | all-to-all | bytes 589824 | tf_op jit(solution)/shard_map/all_to_all | solution.py:21
  108.9 11.6 %all_to_all.39 = f32[32,1,128]{2,1,0:T(1,128)S(1)} all-to-all(f32[32,1,128]{2,1,0:T(1,128)S(1)} %broadcast_in_dim.26), channel_id=1, replica_groups=mesh['z'=8,'y_high'=2,'y_low'=2,'cb'=8] {'z','y_high','y_low'}, dimensions={0} | all-to-all | bytes 32768 | tf_op jit(solution)/shard_map/all_to_all | solution.py:21
  120.5 0.6 fusion.7
  (37 shorter events, 0.7 us)
Async XLA Ops:
  3.6 12.2 %copy-start = (bf16[64,1408]{1,0:T(8,128)(2,1)S(1)}, bf16[64,1408]{1,0:T(8,128)(2,1)}, u32[]{:S(2)}) copy-start(bf16[64,1408]{1,0:T(8,128)(2,1)} %get-tuple-element.22) | copy-start | bytes 540676
  3.6 26.0 %all-to-all-start = ((bf16[32,48,128]{2,1,0:T(8,128)(2,1)}), bf16[32,48,128]{2,1,0:T(8,128)(2,1)S(1)}, u32[]{:S(2)}, u32[]{:S(2)}) async-start(bf16[32,48,128]{2,1,0:T(8,128)(2,1)} %get-tuple-element.21), calls=%async_computation | async-start | bytes 786432 | tf_op jit(solution)/shard_map/all_to_all | solution.py:21
  45.6 7.5 %copy-start.1 = (bf16[64,1408]{1,0:T(8,128)(2,1)S(1)}, bf16[64,1408]{1,0:T(8,128)(2,1)}, u32[]{:S(2)}) copy-start(bf16[64,1408]{1,0:T(8,128)(2,1)} %get-tuple-element.26) | copy-start | bytes 540676
  45.6 15.0 %all-to-all-start.2 = ((f16[16,72,128]{2,1,0:T(8,128)(2,1)}), f16[16,72,128]{2,1,0:T(8,128)(2,1)S(1)}, u32[]{:S(2)}, u32[]{:S(2)}) async-start(f16[16,72,128]{2,1,0:T(8,128)(2,1)} %broadcast_in_dim.20), calls=%async_computation.2 | async-start | bytes 589824 | tf_op jit(solution)/shard_map/all_to_all | solution.py:21
  53.1 9.2 %collective-permute-start = (bf16[64,1408]{1,0:T(8,128)(2,1)S(1)}, bf16[64,1408]{1,0:T(8,128)(2,1)S(1)}, u32[]{:S(2)}, u32[]{:S(2)}) collective-permute-start(bf16[64,1408]{1,0:T(8,128)(2,1)S(1)} %copy-done.1), channel_id=1, source_target_pairs={{0,8},{8,0},{1,9},{9,1},{2,10},{10,2},{3,11},{11,3},{4,12},{12,4},... | collective-permute-start | bytes 540680 | tf_op jit(solution)/shard_map/ppermute | solution.py:208

commit v4 on v3

--- a/solution.py
+++ b/solution.py
@@ -96,14 +96,13 @@
 
 
 def first_kernel(*refs):
-    sources, (out_ref, keep_out_ref, give_out_ref, *refs) = refs[:6], refs[6:]
-    flat_ref, stage_ref, tiles_ref, keep_ref, give_ref, turn_ref, *held, in_sems, out_sems = refs
-    pieces = [*sources[:3], sources[3].at[0], sources[4].at[0], *[source.at[1] for source in sources[3:]]]
-    copies = [pltpu.make_async_copy(pieces[i], held[i], in_sems.at[i]) for i in range(8)]
+    sources, (out_ref, flat_ref, stage_ref, tiles_ref, *held, in_sems, out_sems) = refs[:4], refs[4:]
+    pieces = [*sources[:2], sources[2].at[0], sources[3].at[0]]
+    copies = [pltpu.make_async_copy(pieces[i], held[i], in_sems.at[i]) for i in range(4)]
     for copy in copies:
         copy.start()
-    tokens_ref, pre_ref, post_ref, gate_ref, up_ref, *traded_refs = held
-    for copy in copies[:3]:
+    tokens_ref, pre_ref, gate_ref, up_ref = held
+    for copy in copies[:2]:
         copy.wait()
     start = tokens_ref[...].astype(f32)
     squares = total(start * start)
@@ -111,9 +110,9 @@
     sums = rows_of([high, squares - high])[:4]
     columns = stacked(start * column(pre_ref[0:1]))
     for k, ref in enumerate((gate_ref, up_ref)):
-        copies[3 + k].wait()
+        copies[2 + k].wait()
         multiply(flat_ref, k, ref[...], columns)
-    n, groups = tiles_ref.shape[0], out_sems.shape[0] - 2
+    n, groups = tiles_ref.shape[0], out_sems.shape[0]
     writes = []
     for g in range(groups):
         part = slice(g * n // groups, (g + 1) * n // groups)
@@ -121,47 +120,77 @@
         tiles_ref[part] = stage_ref[part].astype(bf16)
         writes.append(pltpu.make_async_copy(tiles_ref.at[part], out_ref.at[part], out_sems.at[g]))
         writes[-1].start()
-
+    for write in writes:
+        write.wait()
+
+
+def first_tiles(n, *operands):
+    (count, ntok), width = operands[0].shape, operands[-1].shape[2]
+    rows, groups = 2 * (width // n) + 4, 2
+    hbm = pl.BlockSpec(memory_space=pltpu.HBM)
+    return pl.pallas_call(
+        first_kernel,
+        out_shape=jax.ShapeDtypeStruct((n, rows, ntok), bf16),
+        in_specs=[hbm] * 4,
+        out_specs=hbm,
+        scratch_shapes=[
+            pltpu.VMEM((2, width, ntok), f32),
+            pltpu.VMEM((n, rows, ntok), f32),
+            pltpu.VMEM((n, rows, ntok), bf16),
+            *[pltpu.VMEM(x.shape, x.dtype) for x in operands[:2]],
+            *[pltpu.VMEM((count, width), bf16) for _ in range(2)],
+            pltpu.SemaphoreType.DMA((4,)),
+            pltpu.SemaphoreType.DMA((groups,)),
+        ],
+    )(*operands)
+
+
+def halves_kernel(*refs):
+    sources, (keep_out_ref, give_out_ref, keep_ref, give_ref, turn_ref, *held, in_sems, out_sems) = refs[:6], refs[6:]
+    pieces = [*sources[:3], *[source.at[1] for source in sources[3:]]]
+    copies = [pltpu.make_async_copy(pieces[i], held[i], in_sems.at[i]) for i in range(6)]
+    for copy in copies:
+        copy.start()
+    tokens_ref, pre_ref, post_ref, *traded_refs = held
     low = lax.axis_index("y_low") == lax.axis_index("y_high")
     width, wide = traded_refs[0].shape[1], turn_ref.shape[1]
-    half, step = width // 2, wide // 2
+    half, step, ntok = width // 2, wide // 2, tokens_ref.shape[1]
+    for copy in copies:
+        copy.wait()
     for k, ref in enumerate(traded_refs):
-        copies[5 + k].wait()
         turn_ref[:, :width] = ref[...].astype(f32)
         first, second = turn_ref[:, :half], pltpu.roll(turn_ref[...], wide - half, 1)[:, :half]
         keep_ref[:, k * step : k * step + half] = jnp.where(low, first, second).astype(bf16)
         give_ref[:, k * step : k * step + half] = jnp.where(low, second, first).astype(bf16)
-    ntok = tokens_ref.shape[1]
     gains = gain_lanes([column(row) for row in (pre_ref[1:2], post_ref[0:1], post_ref[1:2])])
     for ref in (keep_ref, give_ref):
         ref[:, 3 * step : 3 * step + ntok] = tokens_ref[...]
         ref[:, 3 * step + ntok :] = gains
+    writes = []
     for i, (source, target) in enumerate(((keep_ref, keep_out_ref), (give_ref, give_out_ref))):
-        writes.append(pltpu.make_async_copy(source, target, out_sems.at[groups + i]))
+        writes.append(pltpu.make_async_copy(source, target, out_sems.at[i]))
         writes[-1].start()
     for write in writes:
         write.wait()
 
 
-def first_tiles(n, *operands):
+def halves_of(*operands):
     (count, ntok), width = operands[0].shape, operands[-1].shape[2]
-    rows, groups, step = 2 * (width // n) + 4, 2, -(-width // 256) * 128
-    outs = [jax.ShapeDtypeStruct(shape, bf16) for shape in ((n, rows, ntok), *[(count, 3 * step + ntok + 128)] * 2)]
+    step = -(-width // 256) * 128
+    out = jax.ShapeDtypeStruct((count, 3 * step + ntok + 128), bf16)
     hbm = pl.BlockSpec(memory_space=pltpu.HBM)
     return pl.pallas_call(
-        first_kernel,
-        out_shape=outs,
+        halves_kernel,
+        out_shape=[out] * 2,
         in_specs=[hbm] * 6,
-        out_specs=[hbm] * 3,
+        out_specs=[hbm] * 2,
         scratch_shapes=[
-            pltpu.VMEM((2, width, ntok), f32),
-            pltpu.VMEM((n, rows, ntok), f32),
-            *[pltpu.VMEM(out.shape, bf16) for out in outs],
+            *[pltpu.VMEM(out.shape, bf16)] * 2,
             pltpu.VMEM((count, 2 * step), f32),
             *[pltpu.VMEM(x.shape, x.dtype) for x in operands[:3]],
-            *[pltpu.VMEM((count, width), bf16) for _ in range(5)],
-            pltpu.SemaphoreType.DMA((8,)),
-            pltpu.SemaphoreType.DMA((groups + 2,)),
+            *[pltpu.VMEM((count, width), bf16) for _ in range(3)],
+            pltpu.SemaphoreType.DMA((6,)),
+            pltpu.SemaphoreType.DMA((2,)),
         ],
     )(*operands)
 
@@ -220,13 +249,15 @@
 
     held = gate_weight.shape[2] // 2
     down_weight = down_weight.transpose(0, 2, 1)
-    tiles, keep, give = first_tiles(n, turned, pre_gain, post_gain, gate_weight, up_weight, down_weight)
-    down_now = jnp.where(low, down_weight[0], down_weight[0] * 1)
-    tiles, low, down_now = lax.optimization_barrier((tiles, low, down_now))
+    tiles = first_tiles(n, turned, pre_gain, gate_weight, up_weight)
+    tiles, low = lax.optimization_barrier((tiles, low))
+    got = exchange(tiles, RA)
+    keep, give = halves_of(turned, pre_gain, post_gain, gate_weight, up_weight, down_weight)
     other = traded(give)
-    got = exchange(tiles, RA)
     step = -(-held // 128) * 128
-    got, keep, side = lax.optimization_barrier((got, keep[:, : 3 * step], keep[:, 3 * step :]))
+    got, keep, side, down_now = lax.optimization_barrier(
+        (got, keep[:, : 3 * step], keep[:, 3 * step :], down_weight[0])
+    )
     got = jnp.sum(got.astype(f32), axis=0)
     squares = total(got[2 * size : 2 * size + 2])
     scale_in = lax.rsqrt(squares / D + EPSILON)

time: 122 us -> 120 us (0.984)
  waiting for transfers between devices: 21.4 us -> 17.7 us
  Pallas kernels: 3.32 us -> 4.88 us
    all_to_all x2, waiting for transfers between devices: 19.8 us -> 16.1 us  [exchange(): lax.all_to_all(tiles, axis, 0, 0, axis_index_groups=groups, tiled=True)]
    pallas_call x1 -> x2, Pallas kernels: 2.7 us -> 4.26 us  [the longest x1 2.23 us: first_tiles(): pl.pallas_call(first_kernel, out_shape=jax.ShapeDtypeStruct((n, rows, nto...]
  transfers between devices with their start and end apart: 3 -> 3, of which waited for: 3 -> 3; matrix products, arithmetic and copies ran while one was open for 0% -> 2% of each run, Pallas kernels for 0% -> 2%
where the time goes in v4:
time: 120 us
  blocking collectives  71.3 us (59%)
  starting transfers between devices  21 us (18%)
  waiting for transfers between devices  17.7 us (15%)
  Pallas kernels  4.88 us (4%)
  local copies, waits for them, and re-layouts  2.71 us (2%)
  other arithmetic  1.32 us (1%)
    all_to_all x5, blocking collectives, exchange(): lax.all_to_all(tiles, axis, 0, 0, axis_index_groups=groups, tiled=True)  71.3 us
    all_to_all x2, starting transfers between devices, exchange(): lax.all_to_all(tiles, axis, 0, 0, axis_index_groups=groups, tiled=True)  19.5 us
    all_to_all x2, waiting for transfers between devices, exchange(): lax.all_to_all(tiles, axis, 0, 0, axis_index_groups=groups, tiled=True)  16.1 us
  transfers between devices with their start and end apart: 3, of which 3 were waited for; matrix products, arithmetic and copies ran while one was open for 2% of the time, Pallas kernels for 2%

profile of v4, /device:TPU:1, one launch (start us, length us, event | category | flops | bytes accessed | tf_op | source)
XLA Modules:
  0.0 119.6 jit_solution(15146072571539568896)
XLA Ops:
  0.0 2.2 %shard_map.64 = bf16[32,48,128]{2,1,0:T(8,128)(2,1)} custom-call(bf16[64,128]{1,0:T(8,128)(2,1)} %bitcast.33, f32[2,64]{1,0:T(2,128)} %refs_1_.3, bf16[2,64,704]{2,1,0:T(8,128)(2,1)} %refs_3_.3, bf16[2,64,704]{2,1,0:T(8,128)(2,1)} %refs_4_.1), custom_call_target="tpu_custom_call" | custom-call | tf_op jit(solution)/shard_map/pallas_call | solution.py:131
  2.2 12.0 %all-to-all-start = ((bf16[32,48,128]{2,1,0:T(8,128)(2,1)}), bf16[32,48,128]{2,1,0:T(8,128)(2,1)S(1)}, u32[]{:S(2)}, u32[]{:S(2)}) async-start(bf16[32,48,128]{2,1,0:T(8,128)(2,1)} %shard_map.64), calls=%async_computation | async-start | bytes 786432 | tf_op jit(solution)/shard_map/all_to_all | solution.py:21
  14.3 2.0 %shard_map.65 = (bf16[64,1408]{1,0:T(8,128)(2,1)}, bf16[64,1408]{1,0:T(8,128)(2,1)}) custom-call(bf16[64,128]{1,0:T(8,128)(2,1)} %bitcast.34, f32[2,64]{1,0:T(2,128)} %refs_1_.3, f32[2,64]{1,0:T(2,128)} %refs_2_.3, bf16[2,64,704]{2,1,0:T(8,128)(2,1)} %refs_3_.3, bf16[2,64,704]{2,1,0:T(8,128)(2,1)} %refs_4_.1, bf16[2,64,704]{2,1,0:T(8,128)(2,1)} %bitcast.31), custom_call_target="tpu_custom_call" | custom-call | tf_op jit(solution)/shard_map/pallas_call | solution.py:182
  16.3 0.0 copy-start
  16.3 1.0 slice.66.refs_1_
  17.3 0.8 slice.67.refs_2_
  18.1 0.0 copy-done
  18.1 10.0 %all-to-all-done = bf16[32,48,128]{2,1,0:T(8,128)(2,1)S(1)} async-done(((bf16[32,48,128]{2,1,0:T(8,128)(2,1)}), bf16[32,48,128]{2,1,0:T(8,128)(2,1)S(1)}, u32[]{:S(2)}, u32[]{:S(2)}) %all-to-all-start) | async-done | bytes 393248 | tf_op jit(solution)/shard_map/all_to_all | solution.py:21
  28.1 0.1 convert_reduce_fusion.1
  28.3 14.8 %all_to_all.35 = bf16[32,22,128]{2,1,0:T(8,128)(2,1)S(1)} all-to-all(bf16[32,22,128]{2,1,0:T(8,128)(2,1)S(1)} %broadcast_in_dim.18), channel_id=1, replica_groups=mesh['z'=8,'y_high'=2,'y_low'=2,'cb'=8] {'z','y_high','y_low'}, dimensions={0} | all-to-all | bytes 360448 | tf_op jit(solution)/shard_map/all_to_all | solution.py:21
  43.0 0.1 reshape.191
  43.1 0.2 abs_reduce_fusion.2
  43.3 0.7 broadcast_in_dim.20
  44.1 0.0 copy-start.1
  44.1 7.5 %all-to-all-start.2 = ((f16[16,72,128]{2,1,0:T(8,128)(2,1)}), f16[16,72,128]{2,1,0:T(8,128)(2,1)S(1)}, u32[]{:S(2)}, u32[]{:S(2)}) async-start(f16[16,72,128]{2,1,0:T(8,128)(2,1)} %broadcast_in_dim.20), calls=%async_computation.2 | async-start | bytes 589824 | tf_op jit(solution)/shard_map/all_to_all | solution.py:21
  51.6 0.0 copy-done.1
  51.6 1.4 %collective-permute-start = (bf16[64,1408]{1,0:T(8,128)(2,1)S(1)}, bf16[64,1408]{1,0:T(8,128)(2,1)S(1)}, u32[]{:S(2)}, u32[]{:S(2)}) collective-permute-start(bf16[64,1408]{1,0:T(8,128)(2,1)S(1)} %copy-done.1), channel_id=1, source_target_pairs={{0,8},{8,0},{1,9},{9,1},{2,10},{10,2},{3,11},{11,3},{4,12},{12,4},... | collective-permute-start | bytes 540680 | tf_op jit(solution)/shard_map/ppermute | solution.py:237
  53.0 6.0 %all-to-all-done.2 = f16[16,72,128]{2,1,0:T(8,128)(2,1)S(1)} async-done(((f16[16,72,128]{2,1,0:T(8,128)(2,1)}), f16[16,72,128]{2,1,0:T(8,128)(2,1)S(1)}, u32[]{:S(2)}, u32[]{:S(2)}) %all-to-all-start.2) | async-done | bytes 294944 | tf_op jit(solution)/shard_map/all_to_all | solution.py:21
  59.2 1.6 %collective-permute-done.refs_3_ = bf16[64,1408]{1,0:T(8,128)(2,1)S(1)} collective-permute-done((bf16[64,1408]{1,0:T(8,128)(2,1)S(1)}, bf16[64,1408]{1,0:T(8,128)(2,1)S(1)}, u32[]{:S(2)}, u32[]{:S(2)}) %collective-permute-start) | collective-permute-done | bytes 180256 | tf_op jit(solution)/shard_map/ppermute | solution.py:237
  60.8 0.6 shard_map.66
  61.5 16.8 %all_to_all.36 = bf16[16,96,128]{2,1,0:T(8,128)(2,1)S(1)} all-to-all(bf16[16,96,128]{2,1,0:T(8,128)(2,1)S(1)} %get-tuple-element.27), channel_id=1, replica_groups={{0,24,32,56,64,88,96,120,128,152,160,184,192,216,224,248},{8,16,40,48,7..., dimensions={0} | all-to-all | bytes 786432 | tf_op jit(solution)/shard_map/all_to_all | solution.py:21
  78.3 0.1 convert_reduce_fusion
  78.5 13.4 %all_to_all.37 = bf16[16,22,128]{2,1,0:T(8,128)(2,1)S(1)} all-to-all(bf16[16,22,128]{2,1,0:T(8,128)(2,1)S(1)} %broadcast_in_dim.21), channel_id=1, replica_groups={{0,24,32,56,64,88,96,120,128,152,160,184,192,216,224,248},{8,16,40,48,7..., dimensions={0} | all-to-all | bytes 180224 | tf_op jit(solution)/shard_map/all_to_all | solution.py:21
  91.9 0.2 abs_reduce_fusion.1
  92.1 0.2 abs_reduce_fusion
  92.4 0.1 pad_maximum_fusion
  92.5 14.7 %all_to_all.38 = f16[16,72,128]{2,1,0:T(8,128)(2,1)S(1)} all-to-all(f16[16,72,128]{2,1,0:T(8,128)(2,1)S(1)} %pad_maximum_fusion), channel_id=1, replica_groups=mesh['z'=8,'y_high'=2,'y_low'=2,'cb'=8] {'y_low','cb'}, dimensions={0} | all-to-all | bytes 589824 | tf_op jit(solution)/shard_map/all_to_all | solution.py:21
  107.3 0.1 fusion
  107.4 11.6 %all_to_all.39 = f32[32,1,128]{2,1,0:T(1,128)S(1)} all-to-all(f32[32,1,128]{2,1,0:T(1,128)S(1)} %broadcast_in_dim.26), channel_id=1, replica_groups=mesh['z'=8,'y_high'=2,'y_low'=2,'cb'=8] {'z','y_high','y_low'}, dimensions={0} | all-to-all | bytes 32768 | tf_op jit(solution)/shard_map/all_to_all | solution.py:21
  119.0 0.6 fusion.7
  (35 shorter events, 0.6 us)
Async XLA Ops:
  2.2 25.9 %all-to-all-start = ((bf16[32,48,128]{2,1,0:T(8,128)(2,1)}), bf16[32,48,128]{2,1,0:T(8,128)(2,1)S(1)}, u32[]{:S(2)}, u32[]{:S(2)}) async-start(bf16[32,48,128]{2,1,0:T(8,128)(2,1)} %shard_map.64), calls=%async_computation | async-start | bytes 786432 | tf_op jit(solution)/shard_map/all_to_all | solution.py:21
  16.3 1.7 %copy-start = (bf16[2,704,64]{1,2,0:T(8,128)(2,1)S(1)}, bf16[2,704,64]{1,2,0:T(8,128)(2,1)}, u32[]{:S(2)}) copy-start(bf16[2,704,64]{1,2,0:T(8,128)(2,1)} %param.11) | copy-start | bytes 540676
  44.1 7.5 %copy-start.1 = (bf16[64,1408]{1,0:T(8,128)(2,1)S(1)}, bf16[64,1408]{1,0:T(8,128)(2,1)}, u32[]{:S(2)}) copy-start(bf16[64,1408]{1,0:T(8,128)(2,1)} %get-tuple-element.24) | copy-start | bytes 540676
  44.1 15.0 %all-to-all-start.2 = ((f16[16,72,128]{2,1,0:T(8,128)(2,1)}), f16[16,72,128]{2,1,0:T(8,128)(2,1)S(1)}, u32[]{:S(2)}, u32[]{:S(2)}) async-start(f16[16,72,128]{2,1,0:T(8,128)(2,1)} %broadcast_in_dim.20), calls=%async_computation.2 | async-start | bytes 589824 | tf_op jit(solution)/shard_map/all_to_all | solution.py:21
  51.6 9.2 %collective-permute-start = (bf16[64,1408]{1,0:T(8,128)(2,1)S(1)}, bf16[64,1408]{1,0:T(8,128)(2,1)S(1)}, u32[]{:S(2)}, u32[]{:S(2)}) collective-permute-start(bf16[64,1408]{1,0:T(8,128)(2,1)S(1)} %copy-done.1), channel_id=1, source_target_pairs={{0,8},{8,0},{1,9},{9,1},{2,10},{10,2},{3,11},{11,3},{4,12},{12,4},... | collective-permute-start | bytes 540680 | tf_op jit(solution)/shard_map/ppermute | solution.py:237

commit v5 on v4

--- a/solution.py
+++ b/solution.py
@@ -146,9 +146,9 @@
 
 
 def halves_kernel(*refs):
-    sources, (keep_out_ref, give_out_ref, keep_ref, give_ref, turn_ref, *held, in_sems, out_sems) = refs[:6], refs[6:]
+    sources, (keep_out_ref, give_out_ref, keep_ref, give_ref, turn_ref, *held, in_sems, out_sems) = refs[:5], refs[5:]
     pieces = [*sources[:3], *[source.at[1] for source in sources[3:]]]
-    copies = [pltpu.make_async_copy(pieces[i], held[i], in_sems.at[i]) for i in range(6)]
+    copies = [pltpu.make_async_copy(pieces[i], held[i], in_sems.at[i]) for i in range(5)]
     for copy in copies:
         copy.start()
     tokens_ref, pre_ref, post_ref, *traded_refs = held
@@ -164,8 +164,8 @@
         give_ref[:, k * step : k * step + half] = jnp.where(low, second, first).astype(bf16)
     gains = gain_lanes([column(row) for row in (pre_ref[1:2], post_ref[0:1], post_ref[1:2])])
     for ref in (keep_ref, give_ref):
-        ref[:, 3 * step : 3 * step + ntok] = tokens_ref[...]
-        ref[:, 3 * step + ntok :] = gains
+        ref[:, 2 * step : 2 * step + ntok] = tokens_ref[...]
+        ref[:, 2 * step + ntok :] = gains
     writes = []
     for i, (source, target) in enumerate(((keep_ref, keep_out_ref), (give_ref, give_out_ref))):
         writes.append(pltpu.make_async_copy(source, target, out_sems.at[i]))
@@ -177,19 +177,19 @@
 def halves_of(*operands):
     (count, ntok), width = operands[0].shape, operands[-1].shape[2]
     step = -(-width // 256) * 128
-    out = jax.ShapeDtypeStruct((count, 3 * step + ntok + 128), bf16)
+    out = jax.ShapeDtypeStruct((count, 2 * step + ntok + 128), bf16)
     hbm = pl.BlockSpec(memory_space=pltpu.HBM)
     return pl.pallas_call(
         halves_kernel,
         out_shape=[out] * 2,
-        in_specs=[hbm] * 6,
+        in_specs=[hbm] * 5,
         out_specs=[hbm] * 2,
         scratch_shapes=[
             *[pltpu.VMEM(out.shape, bf16)] * 2,
             pltpu.VMEM((count, 2 * step), f32),
             *[pltpu.VMEM(x.shape, x.dtype) for x in operands[:3]],
-            *[pltpu.VMEM((count, width), bf16) for _ in range(3)],
-            pltpu.SemaphoreType.DMA((6,)),
+            *[pltpu.VMEM((count, width), bf16) for _ in range(2)],
+            pltpu.SemaphoreType.DMA((5,)),
             pltpu.SemaphoreType.DMA((2,)),
         ],
     )(*operands)
@@ -198,8 +198,8 @@
 def second_kernel(*refs):
     branch_ref, mine_ref, side_ref, other_ref, out_ref, start_ref, gained_ref, last_ref, flat_ref, stage_ref = refs
     width, ntok = gained_ref.shape
-    held, step = flat_ref.shape[1], mine_ref.shape[1] // 3
-    sides = side_ref[...], other_ref[:, 3 * step :]
+    held, step = flat_ref.shape[1], mine_ref.shape[1] // 2
+    sides = side_ref[...], other_ref[:, 2 * step :]
     start = jnp.concatenate([side[:, :ntok] for side in sides]).astype(f32)
     start_ref[...] = start[:width]
     gains = [jnp.concatenate([gain_of(side[:, ntok:], i) for side in sides]) for i in range(3)]
@@ -252,11 +252,11 @@
     tiles = first_tiles(n, turned, pre_gain, gate_weight, up_weight)
     tiles, low = lax.optimization_barrier((tiles, low))
     got = exchange(tiles, RA)
-    keep, give = halves_of(turned, pre_gain, post_gain, gate_weight, up_weight, down_weight)
+    keep, give = halves_of(turned, pre_gain, post_gain, gate_weight, up_weight)
     other = traded(give)
     step = -(-held // 128) * 128
-    got, keep, side, down_now = lax.optimization_barrier(
-        (got, keep[:, : 3 * step], keep[:, 3 * step :], down_weight[0])
+    got, keep, side, down_now, down_next = lax.optimization_barrier(
+        (got, keep[:, : 2 * step], keep[:, 2 * step :], down_weight[0], down_weight[1])
     )
     got = jnp.sum(got.astype(f32), axis=0)
     squares = total(got[2 * size : 2 * size + 2])
@@ -280,11 +280,8 @@
     stream = RESIDUAL * start + gained * scale_out
 
     both = (RESIDUAL * got[2 * size : 4 * size] + scale_out * got[: 2 * size]) * scale_in
-    hidden = hidden_of(both, PARTS)
-    halves = pair(*[coded(down_project(x[:, 2 * step : 2 * step + held], hidden)) for x in (keep, other)])
-    members = lax.axis_size("cb")
-    parts = jnp.concatenate([jnp.broadcast_to(half[None], (members, *half.shape)) for half in halves])
-    branch = jnp.sum(decoded(exchange(parts, SUM)), axis=0)
+    hidden = hidden_of(both, [PARTS[0] + PARTS[1]])
+    branch = jnp.sum(decoded(to_all(coded(down_project(down_next, hidden)), "cb")), axis=0)
     branch_sq = jnp.sum(to_all(total(branch * branch), RA), axis=0)
     scale_out = lax.rsqrt(branch_sq / D + EPSILON)
     stream = RESIDUAL * stream + branch * last * scale_out

time: 120 us -> 118 us (0.983)
  no operation moved by 1% of the time
where the time goes in v5:
time: 118 us; the launch traced here: 117 us
  blocking collectives  70.4 us (60%)
  starting transfers between devices  21 us (18%)
  waiting for transfers between devices  16.7 us (14%)
  Pallas kernels  4.78 us (4%)
  local copies, waits for them, and re-layouts  2.69 us (2%)
    all_to_all x5, blocking collectives, exchange(): lax.all_to_all(tiles, axis, 0, 0, axis_index_groups=groups, tiled=True)  70.4 us
    all_to_all x2, starting transfers between devices, exchange(): lax.all_to_all(tiles, axis, 0, 0, axis_index_groups=groups, tiled=True)  19.5 us
    all_to_all x2, waiting for transfers between devices, exchange(): lax.all_to_all(tiles, axis, 0, 0, axis_index_groups=groups, tiled=True)  16.2 us
  transfers between devices with their start and end apart: 3, of which 3 were waited for; matrix products, arithmetic and copies ran while one was open for 2% of the time, Pallas kernels for 2%

profile of v5, /device:TPU:1, one launch (start us, length us, event | category | flops | bytes accessed | tf_op | source)
XLA Modules:
  0.0 117.3 jit_solution(12946526418701163468)
XLA Ops:
  0.0 2.2 %shard_map.64 = bf16[32,48,128]{2,1,0:T(8,128)(2,1)} custom-call(bf16[64,128]{1,0:T(8,128)(2,1)} %bitcast.34, f32[2,64]{1,0:T(2,128)} %refs_1_.3, bf16[2,64,704]{2,1,0:T(8,128)(2,1)} %refs_3_.3, bf16[2,64,704]{2,1,0:T(8,128)(2,1)} %refs_4_.1), custom_call_target="tpu_custom_call" | custom-call | tf_op jit(solution)/shard_map/pallas_call | solution.py:131
  2.2 12.0 %all-to-all-start = ((bf16[32,48,128]{2,1,0:T(8,128)(2,1)}), bf16[32,48,128]{2,1,0:T(8,128)(2,1)S(1)}, u32[]{:S(2)}, u32[]{:S(2)}) async-start(bf16[32,48,128]{2,1,0:T(8,128)(2,1)} %shard_map.64), calls=%async_computation | async-start | bytes 786432 | tf_op jit(solution)/shard_map/all_to_all | solution.py:21
  14.3 1.9 %shard_map.65 = (bf16[64,1024]{1,0:T(8,128)(2,1)}, bf16[64,1024]{1,0:T(8,128)(2,1)}) custom-call(bf16[64,128]{1,0:T(8,128)(2,1)} %bitcast.35, f32[2,64]{1,0:T(2,128)} %refs_1_.3, f32[2,64]{1,0:T(2,128)} %refs_2_.3, bf16[2,64,704]{2,1,0:T(8,128)(2,1)} %refs_3_.3, bf16[2,64,704]{2,1,0:T(8,128)(2,1)} %refs_4_.1), custom_call_target="tpu_custom_call" | custom-call | tf_op jit(solution)/shard_map/pallas_call | solution.py:182
  16.2 0.0 copy-start
  16.2 0.9 slice.63.refs_1_
  17.2 0.8 slice.64.refs_2_
  17.9 0.0 copy-done
  17.9 10.2 %all-to-all-done = bf16[32,48,128]{2,1,0:T(8,128)(2,1)S(1)} async-done(((bf16[32,48,128]{2,1,0:T(8,128)(2,1)}), bf16[32,48,128]{2,1,0:T(8,128)(2,1)S(1)}, u32[]{:S(2)}, u32[]{:S(2)}) %all-to-all-start) | async-done | bytes 393248 | tf_op jit(solution)/shard_map/all_to_all | solution.py:21
  28.1 0.1 convert_reduce_fusion.1
  28.3 14.8 %all_to_all.35 = bf16[32,22,128]{2,1,0:T(8,128)(2,1)S(1)} all-to-all(bf16[32,22,128]{2,1,0:T(8,128)(2,1)S(1)} %broadcast_in_dim.14), channel_id=1, replica_groups=mesh['z'=8,'y_high'=2,'y_low'=2,'cb'=8] {'z','y_high','y_low'}, dimensions={0} | all-to-all | bytes 360448 | tf_op jit(solution)/shard_map/all_to_all | solution.py:21
  43.0 0.1 reshape.121
  43.1 0.2 abs_reduce_fusion.1
  43.3 0.7 broadcast_in_dim.16
  44.1 0.0 copy-start.1
  44.1 7.5 %all-to-all-start.2 = ((f16[16,72,128]{2,1,0:T(8,128)(2,1)}), f16[16,72,128]{2,1,0:T(8,128)(2,1)S(1)}, u32[]{:S(2)}, u32[]{:S(2)}) async-start(f16[16,72,128]{2,1,0:T(8,128)(2,1)} %broadcast_in_dim.16), calls=%async_computation.2 | async-start | bytes 589824 | tf_op jit(solution)/shard_map/all_to_all | solution.py:21
  51.6 0.0 copy-done.1
  51.6 1.4 %collective-permute-start = (bf16[64,1024]{1,0:T(8,128)(2,1)S(1)}, bf16[64,1024]{1,0:T(8,128)(2,1)S(1)}, u32[]{:S(2)}, u32[]{:S(2)}) collective-permute-start(bf16[64,1024]{1,0:T(8,128)(2,1)S(1)} %copy-done.1), channel_id=1, source_target_pairs={{0,8},{8,0},{1,9},{9,1},{2,10},{10,2},{3,11},{11,3},{4,12},{12,4},... | collective-permute-start | bytes 393224 | tf_op jit(solution)/shard_map/ppermute | solution.py:237
  53.0 6.0 %all-to-all-done.2 = f16[16,72,128]{2,1,0:T(8,128)(2,1)S(1)} async-done(((f16[16,72,128]{2,1,0:T(8,128)(2,1)}), f16[16,72,128]{2,1,0:T(8,128)(2,1)S(1)}, u32[]{:S(2)}, u32[]{:S(2)}) %all-to-all-start.2) | async-done | bytes 294944 | tf_op jit(solution)/shard_map/all_to_all | solution.py:21
  59.2 0.6 collective-permute-done.refs_3_
  59.8 0.6 shard_map.66
  60.4 16.8 %all_to_all.36 = bf16[16,96,128]{2,1,0:T(8,128)(2,1)S(1)} all-to-all(bf16[16,96,128]{2,1,0:T(8,128)(2,1)S(1)} %get-tuple-element.28), channel_id=1, replica_groups={{0,24,32,56,64,88,96,120,128,152,160,184,192,216,224,248},{8,16,40,48,7..., dimensions={0} | all-to-all | bytes 786432 | tf_op jit(solution)/shard_map/all_to_all | solution.py:21
  77.3 0.1 convert_reduce_fusion
  77.4 13.9 %all_to_all.37 = bf16[32,22,128]{2,1,0:T(8,128)(2,1)S(1)} all-to-all(bf16[32,22,128]{2,1,0:T(8,128)(2,1)S(1)} %broadcast_in_dim.17), channel_id=1, replica_groups={{0,24,32,56,64,88,96,120,128,152,160,184,192,216,224,248,8,16,40,48,72,..., dimensions={0} | all-to-all | bytes 360448 | tf_op jit(solution)/shard_map/all_to_all | solution.py:21
  91.3 0.1 reshape.123
  91.4 0.2 abs_reduce_fusion
  91.7 12.9 %all_to_all.38 = f16[8,72,128]{2,1,0:T(8,128)(2,1)S(1)} all-to-all(f16[8,72,128]{2,1,0:T(8,128)(2,1)S(1)} %broadcast_in_dim.19), channel_id=1, replica_groups=mesh['z'=8,'y_high'=2,'y_low'=2,'cb'=8] {'cb'}, dimensions={0} | all-to-all | bytes 294912 | tf_op jit(solution)/shard_map/all_to_all | solution.py:21
  104.7 11.9 %all_to_all.39 = f32[32,1,128]{2,1,0:T(1,128)S(1)} all-to-all(f32[32,1,128]{2,1,0:T(1,128)S(1)} %broadcast_in_dim.20), channel_id=1, replica_groups=mesh['z'=8,'y_high'=2,'y_low'=2,'cb'=8] {'z','y_high','y_low'}, dimensions={0} | all-to-all | bytes 32768 | tf_op jit(solution)/shard_map/all_to_all | solution.py:21
  116.7 0.6 fusion.3
  (32 shorter events, 0.5 us)
Async XLA Ops:
  2.2 25.9 %all-to-all-start = ((bf16[32,48,128]{2,1,0:T(8,128)(2,1)}), bf16[32,48,128]{2,1,0:T(8,128)(2,1)S(1)}, u32[]{:S(2)}, u32[]{:S(2)}) async-start(bf16[32,48,128]{2,1,0:T(8,128)(2,1)} %shard_map.64), calls=%async_computation | async-start | bytes 786432 | tf_op jit(solution)/shard_map/all_to_all | solution.py:21
  16.2 1.7 %copy-start = (bf16[2,704,64]{1,2,0:T(8,128)(2,1)S(1)}, bf16[2,704,64]{1,2,0:T(8,128)(2,1)}, u32[]{:S(2)}) copy-start(bf16[2,704,64]{1,2,0:T(8,128)(2,1)} %param.11) | copy-start | bytes 540676
  44.1 7.5 %copy-start.1 = (bf16[64,1024]{1,0:T(8,128)(2,1)S(1)}, bf16[64,1024]{1,0:T(8,128)(2,1)}, u32[]{:S(2)}) copy-start(bf16[64,1024]{1,0:T(8,128)(2,1)} %get-tuple-element.25) | copy-start | bytes 393220
  44.1 15.0 %all-to-all-start.2 = ((f16[16,72,128]{2,1,0:T(8,128)(2,1)}), f16[16,72,128]{2,1,0:T(8,128)(2,1)S(1)}, u32[]{:S(2)}, u32[]{:S(2)}) async-start(f16[16,72,128]{2,1,0:T(8,128)(2,1)} %broadcast_in_dim.16), calls=%async_computation.2 | async-start | bytes 589824 | tf_op jit(solution)/shard_map/all_to_all | solution.py:21
  51.6 8.2 %collective-permute-start = (bf16[64,1024]{1,0:T(8,128)(2,1)S(1)}, bf16[64,1024]{1,0:T(8,128)(2,1)S(1)}, u32[]{:S(2)}, u32[]{:S(2)}) collective-permute-start(bf16[64,1024]{1,0:T(8,128)(2,1)S(1)} %copy-done.1), channel_id=1, source_target_pairs={{0,8},{8,0},{1,9},{9,1},{2,10},{10,2},{3,11},{11,3},{4,12},{12,4},... | collective-permute-start | bytes 393224 | tf_op jit(solution)/shard_map/ppermute | solution.py:237

commit v6 on v5

--- a/solution.py
+++ b/solution.py
@@ -14,7 +14,7 @@
 bf16 = jnp.bfloat16
 RA = ("z", "y_high", "y_low")
 PARTS = [[4 * z + y for z in range(8) for y in ys] for ys in ((0, 3), (1, 2))]
-SUM = ("y_low", "cb")
+CB = ("chip", "core")
 
 
 def exchange(tiles, axis, groups=None):
@@ -267,7 +267,9 @@
         return to_all(hidden, RA, groups).reshape(-1, ntok)
 
     hidden = hidden_of(got[: 2 * size] * scale_in, None)
-    parts = decoded(to_all(coded(down_project(down_now, hidden)), SUM))
+    part = down_project(down_now, hidden)
+    part = part + lax.ppermute(part, "core", [(0, 1), (1, 0)])
+    parts = decoded(to_all(coded(part), ("y_low", "chip")))
     branch = jnp.concatenate(pair(*jnp.sum(parts.reshape(2, -1, width, ntok), axis=1)))
 
     tiles, start, gained, last = second_tiles(n // 2, held, branch, keep, side, other)
@@ -281,7 +283,7 @@
 
     both = (RESIDUAL * got[2 * size : 4 * size] + scale_out * got[: 2 * size]) * scale_in
     hidden = hidden_of(both, [PARTS[0] + PARTS[1]])
-    branch = jnp.sum(decoded(to_all(coded(down_project(down_next, hidden)), "cb")), axis=0)
+    branch = jnp.sum(decoded(to_all(coded(down_project(down_next, hidden)), CB)), axis=0)
     branch_sq = jnp.sum(to_all(total(branch * branch), RA), axis=0)
     scale_out = lax.rsqrt(branch_sq / D + EPSILON)
     stream = RESIDUAL * stream + branch * last * scale_out
@@ -289,11 +291,11 @@
 
 
 def solution(mesh):
-    split = Mesh(mesh.devices.reshape(8, 2, 2, mesh.shape["cb"]), ("z", "y_high", "y_low", "cb"))
+    split = Mesh(mesh.devices.reshape(8, 2, 2, mesh.shape["cb"] // 2, 2), ("z", "y_high", "y_low", "chip", "core"))
     return jax.shard_map(
         sublayers,
         mesh=split,
-        in_specs=(P(None, RA), P(None, RA), P(None, RA), P(None, RA, "cb"), P(None, RA, "cb"), P(None, "cb", RA)),
+        in_specs=(P(None, RA), P(None, RA), P(None, RA), P(None, RA, CB), P(None, RA, CB), P(None, CB, RA)),
         out_specs=P(None, RA),
         check_vma=False,
     )

time: 118 us -> 117 us (level)
  waiting for transfers between devices: 16.7 us -> 15.1 us
    all_to_all x2, starting transfers between devices: 19.5 us -> 16.2 us  [exchange(): lax.all_to_all(tiles, axis, 0, 0, axis_index_groups=groups, tiled=True)]
    ppermute x0 -> x1, starting transfers between devices: none -> 3.14 us  [sublayers(): part = part + lax.ppermute(part, 'core', [(0, 1), (1, 0)])]
    all_to_all x2, waiting for transfers between devices: 16.2 us -> 14.2 us  [exchange(): lax.all_to_all(tiles, axis, 0, 0, axis_index_groups=groups, tiled=True)]
  transfers between devices with their start and end apart: 3 -> 4, of which waited for: 3 -> 3; matrix products, arithmetic and copies ran while one was open for 2% -> 2% of each run, Pallas kernels for 2% -> 2%
where the time goes in v6:
time: 117 us; the launch traced here: 116 us
  blocking collectives  71.1 us (61%)
  starting transfers between devices  20.8 us (18%)
  waiting for transfers between devices  15.1 us (13%)
  Pallas kernels  4.78 us (4%)
  local copies, waits for them, and re-layouts  2.62 us (2%)
    all_to_all x5, blocking collectives, exchange(): lax.all_to_all(tiles, axis, 0, 0, axis_index_groups=groups, tiled=True)  71.1 us
    all_to_all x2, starting transfers between devices, exchange(): lax.all_to_all(tiles, axis, 0, 0, axis_index_groups=groups, tiled=True)  16.2 us
    all_to_all x2, waiting for transfers between devices, exchange(): lax.all_to_all(tiles, axis, 0, 0, axis_index_groups=groups, tiled=True)  14.2 us
    ppermute x1, starting transfers between devices, sublayers(): part = part + lax.ppermute(part, 'core', [(0, 1), (1, 0)])  3.14 us
  transfers between devices with their start and end apart: 4, of which 3 were waited for; matrix products, arithmetic and copies ran while one was open for 2% of the time, Pallas kernels for 2%

profile of v6, /device:TPU:1, one launch (start us, length us, event | category | flops | bytes accessed | tf_op | source)
XLA Modules:
  0.0 116.1 jit_solution(4180523334770822086)
XLA Ops:
  0.0 2.2 %shard_map.64 = bf16[32,48,128]{2,1,0:T(8,128)(2,1)} custom-call(bf16[64,128]{1,0:T(8,128)(2,1)} %bitcast.34, f32[2,64]{1,0:T(2,128)} %refs_1_.3, bf16[2,64,704]{2,1,0:T(8,128)(2,1)} %refs_3_.3, bf16[2,64,704]{2,1,0:T(8,128)(2,1)} %refs_4_.1), custom_call_target="tpu_custom_call" | custom-call | tf_op jit(solution)/shard_map/pallas_call | solution.py:131
  2.2 12.0 %all-to-all-start = ((bf16[32,48,128]{2,1,0:T(8,128)(2,1)}), bf16[32,48,128]{2,1,0:T(8,128)(2,1)S(1)}, u32[]{:S(2)}, u32[]{:S(2)}) async-start(bf16[32,48,128]{2,1,0:T(8,128)(2,1)} %shard_map.64), calls=%async_computation | async-start | bytes 786432 | tf_op jit(solution)/shard_map/all_to_all | solution.py:21
  14.3 1.9 %shard_map.65 = (bf16[64,1024]{1,0:T(8,128)(2,1)}, bf16[64,1024]{1,0:T(8,128)(2,1)}) custom-call(bf16[64,128]{1,0:T(8,128)(2,1)} %bitcast.35, f32[2,64]{1,0:T(2,128)} %refs_1_.3, f32[2,64]{1,0:T(2,128)} %refs_2_.3, bf16[2,64,704]{2,1,0:T(8,128)(2,1)} %refs_3_.3, bf16[2,64,704]{2,1,0:T(8,128)(2,1)} %refs_4_.1), custom_call_target="tpu_custom_call" | custom-call | tf_op jit(solution)/shard_map/pallas_call | solution.py:182
  16.2 0.0 copy-start
  16.2 0.9 slice.63.refs_1_
  17.2 0.8 slice.64.refs_2_
  17.9 0.0 copy-done
  17.9 10.2 %all-to-all-done = bf16[32,48,128]{2,1,0:T(8,128)(2,1)S(1)} async-done(((bf16[32,48,128]{2,1,0:T(8,128)(2,1)}), bf16[32,48,128]{2,1,0:T(8,128)(2,1)S(1)}, u32[]{:S(2)}, u32[]{:S(2)}) %all-to-all-start) | async-done | bytes 393248 | tf_op jit(solution)/shard_map/all_to_all | solution.py:21
  28.1 0.1 convert_reduce_fusion.1
  28.3 14.8 %all_to_all.35 = bf16[32,22,128]{2,1,0:T(8,128)(2,1)S(1)} all-to-all(bf16[32,22,128]{2,1,0:T(8,128)(2,1)S(1)} %broadcast_in_dim.14), channel_id=1, replica_groups=mesh['z'=8,'y_high'=2,'y_low'=2,'chip'=4,'core'=2] {'z','y_high','y_low'}, dimensions={0} | all-to-all | bytes 360448 | tf_op jit(solution)/shard_map/all_to_all | solution.py:21
  43.0 0.1 reshape.121
  43.1 0.2 fusion.13
  43.3 3.1 %collective-permute-start = (f32[64,128]{1,0:T(8,128)S(1)}, f32[64,128]{1,0:T(8,128)S(1)}, u32[]{:S(2)}, u32[]{:S(2)}) collective-permute-start(f32[64,128]{1,0:T(8,128)S(1)} %fusion.13), channel_id=1, source_target_pairs={{0,1},{1,0},{2,3},{3,2},{4,5},{5,4},{6,7},{7,6},{8,9},{9,8},{10,11... | collective-permute-start | bytes 98312 | tf_op jit(solution)/shard_map/ppermute | solution.py:271
  46.4 0.9 collective-permute-done
  47.3 0.7 broadcast_in_dim.16
  48.0 0.0 copy-start.1
  48.0 4.2 %all-to-all-start.2 = ((f16[8,72,128]{2,1,0:T(8,128)(2,1)}), f16[8,72,128]{2,1,0:T(8,128)(2,1)S(1)}, u32[]{:S(2)}, u32[]{:S(2)}) async-start(f16[8,72,128]{2,1,0:T(8,128)(2,1)} %broadcast_in_dim.16), calls=%async_computation.2 | async-start | bytes 294912 | tf_op jit(solution)/shard_map/all_to_all | solution.py:21
  52.2 0.0 copy-done.1
  52.2 1.5 %collective-permute-start.1 = (bf16[64,1024]{1,0:T(8,128)(2,1)S(1)}, bf16[64,1024]{1,0:T(8,128)(2,1)S(1)}, u32[]{:S(2)}, u32[]{:S(2)}) collective-permute-start(bf16[64,1024]{1,0:T(8,128)(2,1)S(1)} %copy-done.1), channel_id=1, source_target_pairs={{0,8},{8,0},{1,9},{9,1},{2,10},{10,2},{3,11},{11,3},{4,12},{12,4},... | collective-permute-start | bytes 393224 | tf_op jit(solution)/shard_map/ppermute | solution.py:237
  53.6 4.1 %all-to-all-done.2 = f16[8,72,128]{2,1,0:T(8,128)(2,1)S(1)} async-done(((f16[8,72,128]{2,1,0:T(8,128)(2,1)}), f16[8,72,128]{2,1,0:T(8,128)(2,1)S(1)}, u32[]{:S(2)}, u32[]{:S(2)}) %all-to-all-start.2) | async-done | bytes 147488 | tf_op jit(solution)/shard_map/all_to_all | solution.py:21
  57.8 0.0 collective-permute-done.1.refs_3_
  57.8 0.6 shard_map.66
  58.5 16.5 %all_to_all.36 = bf16[16,96,128]{2,1,0:T(8,128)(2,1)S(1)} all-to-all(bf16[16,96,128]{2,1,0:T(8,128)(2,1)S(1)} %get-tuple-element.28), channel_id=1, replica_groups={{0,24,32,56,64,88,96,120,128,152,160,184,192,216,224,248},{8,16,40,48,7..., dimensions={0} | all-to-all | bytes 786432 | tf_op jit(solution)/shard_map/all_to_all | solution.py:21
  75.0 0.1 convert_reduce_fusion
  75.2 13.5 %all_to_all.37 = bf16[32,22,128]{2,1,0:T(8,128)(2,1)S(1)} all-to-all(bf16[32,22,128]{2,1,0:T(8,128)(2,1)S(1)} %broadcast_in_dim.17), channel_id=1, replica_groups={{0,24,32,56,64,88,96,120,128,152,160,184,192,216,224,248,8,16,40,48,72,..., dimensions={0} | all-to-all | bytes 360448 | tf_op jit(solution)/shard_map/all_to_all | solution.py:21
  88.7 0.1 reshape.123
  88.8 0.2 abs_reduce_fusion
  89.1 14.4 %all_to_all.38 = f16[8,72,128]{2,1,0:T(8,128)(2,1)S(1)} all-to-all(f16[8,72,128]{2,1,0:T(8,128)(2,1)S(1)} %broadcast_in_dim.19), channel_id=1, replica_groups=mesh['z'=8,'y_high'=2,'y_low'=2,'chip'=4,'core'=2] {'chip','core'}, dimensions={0} | all-to-all | bytes 294912 | tf_op jit(solution)/shard_map/all_to_all | solution.py:21
  103.5 11.9 %all_to_all.39 = f32[32,1,128]{2,1,0:T(1,128)S(1)} all-to-all(f32[32,1,128]{2,1,0:T(1,128)S(1)} %broadcast_in_dim.20), channel_id=1, replica_groups=mesh['z'=8,'y_high'=2,'y_low'=2,'chip'=4,'core'=2] {'z','y_high','y_low'}, dimensions={0} | all-to-all | bytes 32768 | tf_op jit(solution)/shard_map/all_to_all | solution.py:21
  115.5 0.6 fusion.3
  (33 shorter events, 0.5 us)
Async XLA Ops:
  2.2 25.9 %all-to-all-start = ((bf16[32,48,128]{2,1,0:T(8,128)(2,1)}), bf16[32,48,128]{2,1,0:T(8,128)(2,1)S(1)}, u32[]{:S(2)}, u32[]{:S(2)}) async-start(bf16[32,48,128]{2,1,0:T(8,128)(2,1)} %shard_map.64), calls=%async_computation | async-start | bytes 786432 | tf_op jit(solution)/shard_map/all_to_all | solution.py:21
  16.2 1.7 %copy-start = (bf16[2,704,64]{1,2,0:T(8,128)(2,1)S(1)}, bf16[2,704,64]{1,2,0:T(8,128)(2,1)}, u32[]{:S(2)}) copy-start(bf16[2,704,64]{1,2,0:T(8,128)(2,1)} %param.11) | copy-start | bytes 540676
  43.3 4.0 %collective-permute-start = (f32[64,128]{1,0:T(8,128)S(1)}, f32[64,128]{1,0:T(8,128)S(1)}, u32[]{:S(2)}, u32[]{:S(2)}) collective-permute-start(f32[64,128]{1,0:T(8,128)S(1)} %fusion.13), channel_id=1, source_target_pairs={{0,1},{1,0},{2,3},{3,2},{4,5},{5,4},{6,7},{7,6},{8,9},{9,8},{10,11... | collective-permute-start | bytes 98312 | tf_op jit(solution)/shard_map/ppermute | solution.py:271
  48.0 4.2 %copy-start.1 = (bf16[64,1024]{1,0:T(8,128)(2,1)S(1)}, bf16[64,1024]{1,0:T(8,128)(2,1)}, u32[]{:S(2)}) copy-start(bf16[64,1024]{1,0:T(8,128)(2,1)} %get-tuple-element.25) | copy-start | bytes 393220
  48.0 9.7 %all-to-all-start.2 = ((f16[8,72,128]{2,1,0:T(8,128)(2,1)}), f16[8,72,128]{2,1,0:T(8,128)(2,1)S(1)}, u32[]{:S(2)}, u32[]{:S(2)}) async-start(f16[8,72,128]{2,1,0:T(8,128)(2,1)} %broadcast_in_dim.16), calls=%async_computation.2 | async-start | bytes 294912 | tf_op jit(solution)/shard_map/all_to_all | solution.py:21
  52.2 5.6 %collective-permute-start.1 = (bf16[64,1024]{1,0:T(8,128)(2,1)S(1)}, bf16[64,1024]{1,0:T(8,128)(2,1)S(1)}, u32[]{:S(2)}, u32[]{:S(2)}) collective-permute-start(bf16[64,1024]{1,0:T(8,128)(2,1)S(1)} %copy-done.1), channel_id=1, source_target_pairs={{0,8},{8,0},{1,9},{9,1},{2,10},{10,2},{3,11},{11,3},{4,12},{12,4},... | collective-permute-start | bytes 393224 | tf_op jit(solution)/shard_map/ppermute | solution.py:237

commit v7 on v6

--- a/solution.py
+++ b/solution.py
@@ -12,8 +12,7 @@
 RESIDUAL = 0.25
 f32 = jnp.float32
 bf16 = jnp.bfloat16
-RA = ("z", "y_high", "y_low")
-PARTS = [[4 * z + y for z in range(8) for y in ys] for ys in ((0, 3), (1, 2))]
+RA = ("z", "y")
 CB = ("chip", "core")
 
 
@@ -145,61 +144,65 @@
     )(*operands)
 
 
-def halves_kernel(*refs):
-    sources, (keep_out_ref, give_out_ref, keep_ref, give_ref, turn_ref, *held, in_sems, out_sems) = refs[:5], refs[5:]
+def quarters_kernel(*refs):
+    sources, outs, (parts_ref, turn_ref, *held, in_sems, out_sems) = refs[:5], refs[5:9], refs[9:]
     pieces = [*sources[:3], *[source.at[1] for source in sources[3:]]]
     copies = [pltpu.make_async_copy(pieces[i], held[i], in_sems.at[i]) for i in range(5)]
     for copy in copies:
         copy.start()
     tokens_ref, pre_ref, post_ref, *traded_refs = held
-    low = lax.axis_index("y_low") == lax.axis_index("y_high")
+    place_y = lax.axis_index("y")
     width, wide = traded_refs[0].shape[1], turn_ref.shape[1]
-    half, step, ntok = width // 2, wide // 2, tokens_ref.shape[1]
+    quarter, step, ntok = width // 4, (parts_ref.shape[2] - 256) // 2, tokens_ref.shape[1]
     for copy in copies:
         copy.wait()
     for k, ref in enumerate(traded_refs):
         turn_ref[:, :width] = ref[...].astype(f32)
-        first, second = turn_ref[:, :half], pltpu.roll(turn_ref[...], wide - half, 1)[:, :half]
-        keep_ref[:, k * step : k * step + half] = jnp.where(low, first, second).astype(bf16)
-        give_ref[:, k * step : k * step + half] = jnp.where(low, second, first).astype(bf16)
+        quarters = [turn_ref[:, :quarter]]
+        quarters += [pltpu.roll(turn_ref[...], wide - i * quarter, 1)[:, :quarter] for i in range(1, 4)]
+        for d in range(4):
+            part = quarters[d]
+            for y in range(1, 4):
+                part = jnp.where(place_y == y, quarters[(y + d) % 4], part)
+            parts_ref[d, :, k * step : k * step + quarter] = part.astype(bf16)
     gains = gain_lanes([column(row) for row in (pre_ref[1:2], post_ref[0:1], post_ref[1:2])])
-    for ref in (keep_ref, give_ref):
-        ref[:, 2 * step : 2 * step + ntok] = tokens_ref[...]
-        ref[:, 2 * step + ntok :] = gains
-    writes = []
-    for i, (source, target) in enumerate(((keep_ref, keep_out_ref), (give_ref, give_out_ref))):
-        writes.append(pltpu.make_async_copy(source, target, out_sems.at[i]))
-        writes[-1].start()
+    for d in range(4):
+        parts_ref[d, :, 2 * step : 2 * step + ntok] = tokens_ref[...]
+        parts_ref[d, :, 2 * step + ntok :] = gains
+    writes = [pltpu.make_async_copy(parts_ref.at[d], outs[d], out_sems.at[d]) for d in range(4)]
+    for write in writes:
+        write.start()
     for write in writes:
         write.wait()
 
 
-def halves_of(*operands):
+def quarters_of(*operands):
     (count, ntok), width = operands[0].shape, operands[-1].shape[2]
-    step = -(-width // 256) * 128
+    step = -(-width // 512) * 128
     out = jax.ShapeDtypeStruct((count, 2 * step + ntok + 128), bf16)
     hbm = pl.BlockSpec(memory_space=pltpu.HBM)
     return pl.pallas_call(
-        halves_kernel,
-        out_shape=[out] * 2,
+        quarters_kernel,
+        out_shape=[out] * 4,
         in_specs=[hbm] * 5,
-        out_specs=[hbm] * 2,
+        out_specs=[hbm] * 4,
         scratch_shapes=[
-            *[pltpu.VMEM(out.shape, bf16)] * 2,
-            pltpu.VMEM((count, 2 * step), f32),
+            pltpu.VMEM((4, *out.shape), bf16),
+            pltpu.VMEM((count, -(-width // 128) * 128), f32),
             *[pltpu.VMEM(x.shape, x.dtype) for x in operands[:3]],
             *[pltpu.VMEM((count, width), bf16) for _ in range(2)],
             pltpu.SemaphoreType.DMA((5,)),
-            pltpu.SemaphoreType.DMA((2,)),
+            pltpu.SemaphoreType.DMA((4,)),
         ],
     )(*operands)
 
 
 def second_kernel(*refs):
-    branch_ref, mine_ref, side_ref, other_ref, out_ref, start_ref, gained_ref, last_ref, flat_ref, stage_ref = refs
+    branch_ref, mine_ref, side_ref, *other_refs = refs[:6]
+    out_ref, start_ref, gained_ref, last_ref, flat_ref, stage_ref = refs[6:]
     width, ntok = gained_ref.shape
     held, step = flat_ref.shape[1], mine_ref.shape[1] // 2
-    sides = side_ref[...], other_ref[:, 2 * step :]
+    sides = [side_ref[...], *[ref[:, 2 * step :] for ref in other_refs]]
     start = jnp.concatenate([side[:, :ntok] for side in sides]).astype(f32)
     start_ref[...] = start[:width]
     gains = [jnp.concatenate([gain_of(side[:, ntok:], i) for side in sides]) for i in range(3)]
@@ -213,7 +216,7 @@
     for i, columns in enumerate((gained, start)):
         columns = stacked(columns * gains[0])
         for k in range(2):
-            weight = jnp.concatenate([ref[:, k * step : k * step + held] for ref in (mine_ref, other_ref)])
+            weight = jnp.concatenate([ref[:, k * step : k * step + held] for ref in (mine_ref, *other_refs)])
             multiply(flat_ref, 2 * i + k, weight, columns)
     place(flat_ref, stage_ref, sums, range(out_ref.shape[0]))
     out_ref[...] = stage_ref[...].astype(bf16)
@@ -233,8 +236,8 @@
     )(*operands)
 
 
-def traded(array):
-    return lax.ppermute(array, "y_low", [(0, 1), (1, 0)])
+def handed(array, d):
+    return lax.ppermute(array, "y", [(i, (i + d) % 4) for i in range(4)])
 
 
 def sublayers(tokens, pre_gain, post_gain, gate_weight, up_weight, down_weight):
@@ -242,18 +245,16 @@
     size = gate_weight.shape[2] // n
     turned = tokens.T
     width, ntok = turned.shape
-    low = lax.axis_index("y_low") == 0
-
-    def pair(first, second):
-        return jnp.where(low, first, second), jnp.where(low, second, first)
-
-    held = gate_weight.shape[2] // 2
+    held = gate_weight.shape[2] // 4
     down_weight = down_weight.transpose(0, 2, 1)
+    turn = ((4 - lax.axis_index("y")) % 4).astype(jnp.uint32)
     tiles = first_tiles(n, turned, pre_gain, gate_weight, up_weight)
-    tiles, low = lax.optimization_barrier((tiles, low))
+    tiles, turn = lax.optimization_barrier((tiles, turn))
     got = exchange(tiles, RA)
-    keep, give = halves_of(turned, pre_gain, post_gain, gate_weight, up_weight)
-    other = traded(give)
+    keep, *gives = quarters_of(turned, pre_gain, post_gain, gate_weight, up_weight)
+    others = []
+    for d, give in enumerate(gives, 1):
+        others.append(handed(give, d))
     step = -(-held // 128) * 128
     got, keep, side, down_now, down_next = lax.optimization_barrier(
         (got, keep[:, : 2 * step], keep[:, 2 * step :], down_weight[0], down_weight[1])
@@ -269,11 +270,13 @@
     hidden = hidden_of(got[: 2 * size] * scale_in, None)
     part = down_project(down_now, hidden)
     part = part + lax.ppermute(part, "core", [(0, 1), (1, 0)])
-    parts = decoded(to_all(coded(part), ("y_low", "chip")))
-    branch = jnp.concatenate(pair(*jnp.sum(parts.reshape(2, -1, width, ntok), axis=1)))
-
-    tiles, start, gained, last = second_tiles(n // 2, held, branch, keep, side, other)
-    got = jnp.sum(exchange(tiles, RA, PARTS).astype(f32), axis=0)
+    parts = decoded(to_all(coded(part), ("y", "chip")))
+    parts = jnp.sum(parts.reshape(4, -1, width, ntok), axis=1)
+    parts = jnp.stack([parts[-i % 4] for i in range(8)])
+    branch = lax.dynamic_slice_in_dim(parts, turn, 4).reshape(4 * width, ntok)
+
+    tiles, start, gained, last = second_tiles(lax.axis_size("z"), held, branch, keep, side, *others)
+    got = jnp.sum(exchange(tiles, "z").astype(f32), axis=0)
     sums = got[4 * size : 4 * size + 3] + got[4 * size + 3 : 4 * size + 6]
     branch_sq, gained_sq, cross = sums[0:1], sums[1:2], sums[2:3]
     scale_out = lax.rsqrt(branch_sq / D + EPSILON)
@@ -282,7 +285,7 @@
     stream = RESIDUAL * start + gained * scale_out
 
     both = (RESIDUAL * got[2 * size : 4 * size] + scale_out * got[: 2 * size]) * scale_in
-    hidden = hidden_of(both, [PARTS[0] + PARTS[1]])
+    hidden = hidden_of(both, [[4 * z + y for y in range(4) for z in range(8)]])
     branch = jnp.sum(decoded(to_all(coded(down_project(down_next, hidden)), CB)), axis=0)
     branch_sq = jnp.sum(to_all(total(branch * branch), RA), axis=0)
     scale_out = lax.rsqrt(branch_sq / D + EPSILON)
@@ -291,7 +294,7 @@
 
 
 def solution(mesh):
-    split = Mesh(mesh.devices.reshape(8, 2, 2, mesh.shape["cb"] // 2, 2), ("z", "y_high", "y_low", "chip", "core"))
+    split = Mesh(mesh.devices.reshape(8, 4, mesh.shape["cb"] // 2, 2), ("z", "y", "chip", "core"))
     return jax.shard_map(
         sublayers,
         mesh=split,

time: 117 us -> 116 us (level)
  blocking collectives: 71.1 us -> 64.2 us
  starting transfers between devices: 20.8 us -> 25.1 us
  waiting for transfers between devices: 15.1 us -> 17 us
    all_to_all x5, blocking collectives: 71.1 us -> 64.2 us  [exchange(): lax.all_to_all(tiles, axis, 0, 0, axis_index_groups=groups, tiled=True)]
    ppermute x1 -> x3, starting transfers between devices: 1.46 us -> 5.02 us  [handed(): return lax.ppermute(array, 'y', [(i, (i + d) % 4) for i in range(4)])]
    ppermute x1 -> x3, waiting for transfers between devices: 0.01 us -> 2.61 us  [handed(): return lax.ppermute(array, 'y', [(i, (i + d) % 4) for i in range(4)])]
  transfers between devices with their start and end apart: 4 -> 6, of which waited for: 3 -> 4; matrix products, arithmetic and copies ran while one was open for 2% -> 2% of each run, Pallas kernels for 2% -> 2%
where the time goes in v7:
time: 116 us
  blocking collectives  64.2 us (55%)
  starting transfers between devices  25.1 us (22%)
  waiting for transfers between devices  17 us (15%)
  Pallas kernels  4.93 us (4%)
  local copies, waits for them, and re-layouts  2.7 us (2%)
    all_to_all x5, blocking collectives, exchange(): lax.all_to_all(tiles, axis, 0, 0, axis_index_groups=groups, tiled=True)  64.2 us
    all_to_all x2, starting transfers between devices, exchange(): lax.all_to_all(tiles, axis, 0, 0, axis_index_groups=groups, tiled=True)  16.9 us
    all_to_all x2, waiting for transfers between devices, exchange(): lax.all_to_all(tiles, axis, 0, 0, axis_index_groups=groups, tiled=True)  13.6 us
    ppermute x3, starting transfers between devices, handed(): return lax.ppermute(array, 'y', [(i, (i + d) % 4) for i in range(4)])  5.02 us
    ppermute x1, starting transfers between devices, sublayers(): part = part + lax.ppermute(part, 'core', [(0, 1), (1, 0)])  3.14 us
    ppermute x3, waiting for transfers between devices, handed(): return lax.ppermute(array, 'y', [(i, (i + d) % 4) for i in range(4)])  2.61 us
  transfers between devices with their start and end apart: 6, of which 4 were waited for; matrix products, arithmetic and copies ran while one was open for 2% of the time, Pallas kernels for 2%

profile of v7, /device:TPU:1, one launch (start us, length us, event | category | flops | bytes accessed | tf_op | source)
XLA Modules:
  0.0 115.7 jit_solution(14766905334617279325)
XLA Ops:
  0.0 2.2 %shard_map.64 = bf16[32,48,128]{2,1,0:T(8,128)(2,1)} custom-call(bf16[64,128]{1,0:T(8,128)(2,1)} %bitcast.32, f32[2,64]{1,0:T(2,128)} %refs_1_.3, bf16[2,64,704]{2,1,0:T(8,128)(2,1)} %refs_3_.3, bf16[2,64,704]{2,1,0:T(8,128)(2,1)} %refs_4_.1), custom_call_target="tpu_custom_call" | custom-call | tf_op jit(solution)/shard_map/pallas_call | solution.py:130
  2.2 12.0 %all-to-all-start = ((bf16[32,48,128]{2,1,0:T(8,128)(2,1)}), bf16[32,48,128]{2,1,0:T(8,128)(2,1)S(1)}, u32[]{:S(2)}, u32[]{:S(2)}) async-start(bf16[32,48,128]{2,1,0:T(8,128)(2,1)} %shard_map.64), calls=%async_computation | async-start | bytes 786432 | tf_op jit(solution)/shard_map/all_to_all | solution.py:20
  14.3 2.0 %shard_map.65 = (bf16[64,768]{1,0:T(8,128)(2,1)}, bf16[64,768]{1,0:T(8,128)(2,1)}, bf16[64,768]{1,0:T(8,128)(2,1)}, bf16[64,768]{1,0:T(8,128)(2,1)}) custom-call(bf16[64,128]{1,0:T(8,128)(2,1)} %bitcast.33, f32[2,64]{1,0:T(2,128)} %refs_1_.3, f32[2,64]{1,0:T(2,128)} %refs_2_.3, bf16[2,64,704]{2,1,0:T(8,128)(2,1)} %refs_3_.3, bf16[2,64,704]{2,1,0:T(8,128)(2,1)} %refs_4_.1), custom_call_target="tpu_custom_call" | custom-call | tf_op jit(solution)/shard_map/pallas_call | solution.py:184
  16.3 0.0 copy-start
  16.4 0.8 slice.80.refs_2_
  17.2 0.8 slice.79.refs_1_
  18.0 0.0 copy-done
  18.0 10.1 %all-to-all-done = bf16[32,48,128]{2,1,0:T(8,128)(2,1)S(1)} async-done(((bf16[32,48,128]{2,1,0:T(8,128)(2,1)}), bf16[32,48,128]{2,1,0:T(8,128)(2,1)S(1)}, u32[]{:S(2)}, u32[]{:S(2)}) %all-to-all-start) | async-done | bytes 393248 | tf_op jit(solution)/shard_map/all_to_all | solution.py:20
  28.1 0.1 convert_reduce_fusion
  28.3 14.8 %all_to_all.35 = bf16[32,22,128]{2,1,0:T(8,128)(2,1)S(1)} all-to-all(bf16[32,22,128]{2,1,0:T(8,128)(2,1)S(1)} %broadcast_in_dim.14), channel_id=1, replica_groups=mesh['z'=8,'y'=4,'chip'=4,'core'=2] {'z','y'}, dimensions={0} | all-to-all | bytes 360448 | tf_op jit(solution)/shard_map/all_to_all | solution.py:20
  43.0 0.1 reshape.120
  43.1 0.2 fusion.13
  43.3 3.1 %collective-permute-start = (f32[64,128]{1,0:T(8,128)S(1)}, f32[64,128]{1,0:T(8,128)S(1)}, u32[]{:S(2)}, u32[]{:S(2)}) collective-permute-start(f32[64,128]{1,0:T(8,128)S(1)} %fusion.13), channel_id=1, source_target_pairs={{0,1},{1,0},{2,3},{3,2},{4,5},{5,4},{6,7},{7,6},{8,9},{9,8},{10,11... | collective-permute-start | bytes 98312 | tf_op jit(solution)/shard_map/ppermute | solution.py:272
  46.4 0.9 collective-permute-done
  47.4 0.7 broadcast_in_dim.16
  48.1 0.0 copy-start.3
  48.1 0.0 copy-start.2
  48.1 0.0 copy-start.1
  48.1 4.9 %all-to-all-start.2 = ((f16[16,72,128]{2,1,0:T(8,128)(2,1)}), f16[16,72,128]{2,1,0:T(8,128)(2,1)S(1)}, u32[]{:S(2)}, u32[]{:S(2)}) async-start(f16[16,72,128]{2,1,0:T(8,128)(2,1)} %broadcast_in_dim.16), calls=%async_computation.2 | async-start | bytes 589824 | tf_op jit(solution)/shard_map/all_to_all | solution.py:20
  53.0 0.0 copy-done.3
  53.0 1.4 %collective-permute-start.1 = (bf16[64,768]{1,0:T(8,128)(2,1)S(1)}, bf16[64,768]{1,0:T(8,128)(2,1)S(1)}, u32[]{:S(2)}, u32[]{:S(2)}) collective-permute-start(bf16[64,768]{1,0:T(8,128)(2,1)S(1)} %copy-done.3), channel_id=1, source_target_pairs={{0,8},{8,16},{16,24},{24,0},{1,9},{9,17},{17,25},{25,1},{2,10},{10... | collective-permute-start | bytes 294920 | tf_op jit(solution)/shard_map/ppermute | solution.py:240
  54.5 0.0 copy-done.2
  54.5 2.4 %collective-permute-start.2 = (bf16[64,768]{1,0:T(8,128)(2,1)S(1)}, bf16[64,768]{1,0:T(8,128)(2,1)S(1)}, u32[]{:S(2)}, u32[]{:S(2)}) collective-permute-start(bf16[64,768]{1,0:T(8,128)(2,1)S(1)} %copy-done.2), channel_id=1, source_target_pairs={{0,16},{8,24},{16,0},{24,8},{1,17},{9,25},{17,1},{25,9},{2,18},{10... | collective-permute-start | bytes 294920 | tf_op jit(solution)/shard_map/ppermute | solution.py:240
  56.9 0.0 copy-done.1
  56.9 1.2 %collective-permute-start.3 = (bf16[64,768]{1,0:T(8,128)(2,1)S(1)}, bf16[64,768]{1,0:T(8,128)(2,1)S(1)}, u32[]{:S(2)}, u32[]{:S(2)}) collective-permute-start(bf16[64,768]{1,0:T(8,128)(2,1)S(1)} %copy-done.1), channel_id=1, source_target_pairs={{0,24},{8,0},{16,8},{24,16},{1,25},{9,1},{17,9},{25,17},{2,26},{10... | collective-permute-start | bytes 294920 | tf_op jit(solution)/shard_map/ppermute | solution.py:240
  58.0 3.5 %all-to-all-done.2 = f16[16,72,128]{2,1,0:T(8,128)(2,1)S(1)} async-done(((f16[16,72,128]{2,1,0:T(8,128)(2,1)}), f16[16,72,128]{2,1,0:T(8,128)(2,1)S(1)}, u32[]{:S(2)}, u32[]{:S(2)}) %all-to-all-start.2) | async-done | bytes 294944 | tf_op jit(solution)/shard_map/all_to_all | solution.py:20
  61.8 0.0 collective-permute-done.1.refs_3_
  61.8 2.6 %collective-permute-done.2.refs_4_ = bf16[64,768]{1,0:T(8,128)(2,1)S(1)} collective-permute-done((bf16[64,768]{1,0:T(8,128)(2,1)S(1)}, bf16[64,768]{1,0:T(8,128)(2,1)S(1)}, u32[]{:S(2)}, u32[]{:S(2)}) %collective-permute-start.2) | collective-permute-done | bytes 98336 | tf_op jit(solution)/shard_map/ppermute | solution.py:240
  64.4 0.0 collective-permute-done.3.refs_5_
  64.4 0.6 shard_map.66
  65.0 11.3 %all_to_all.36 = bf16[8,96,128]{2,1,0:T(8,128)(2,1)S(1)} all-to-all(bf16[8,96,128]{2,1,0:T(8,128)(2,1)S(1)} %get-tuple-element.32), channel_id=1, replica_groups=mesh['z'=8,'y'=4,'chip'=4,'core'=2] {'z'}, dimensions={0} | all-to-all | bytes 393216 | tf_op jit(solution)/shard_map/all_to_all | solution.py:20
  76.5 14.4 %all_to_all.37 = bf16[32,22,128]{2,1,0:T(8,128)(2,1)S(1)} all-to-all(bf16[32,22,128]{2,1,0:T(8,128)(2,1)S(1)} %broadcast_in_dim.17), channel_id=1, replica_groups={{0,32,64,96,128,160,192,224,8,40,72,104,136,168,200,232,16,48,80,112,14..., dimensions={0} | all-to-all | bytes 360448 | tf_op jit(solution)/shard_map/all_to_all | solution.py:20
  90.9 0.1 reshape.123
  90.9 0.2 abs_reduce_fusion
  91.2 11.5 %all_to_all.38 = f16[8,72,128]{2,1,0:T(8,128)(2,1)S(1)} all-to-all(f16[8,72,128]{2,1,0:T(8,128)(2,1)S(1)} %broadcast_in_dim.19), channel_id=1, replica_groups=mesh['z'=8,'y'=4,'chip'=4,'core'=2] {'chip','core'}, dimensions={0} | all-to-all | bytes 294912 | tf_op jit(solution)/shard_map/all_to_all | solution.py:20
  102.8 12.3 %all_to_all.39 = f32[32,1,128]{2,1,0:T(1,128)S(1)} all-to-all(f32[32,1,128]{2,1,0:T(1,128)S(1)} %broadcast_in_dim.20), channel_id=1, replica_groups=mesh['z'=8,'y'=4,'chip'=4,'core'=2] {'z','y'}, dimensions={0} | all-to-all | bytes 32768 | tf_op jit(solution)/shard_map/all_to_all | solution.py:20
  115.1 0.6 fusion.3
  (41 shorter events, 0.6 us)
Async XLA Ops:
  2.2 25.9 %all-to-all-start = ((bf16[32,48,128]{2,1,0:T(8,128)(2,1)}), bf16[32,48,128]{2,1,0:T(8,128)(2,1)S(1)}, u32[]{:S(2)}, u32[]{:S(2)}) async-start(bf16[32,48,128]{2,1,0:T(8,128)(2,1)} %shard_map.64), calls=%async_computation | async-start | bytes 786432 | tf_op jit(solution)/shard_map/all_to_all | solution.py:20
  16.3 1.7 %copy-start = (bf16[2,704,64]{1,2,0:T(8,128)(2,1)S(1)}, bf16[2,704,64]{1,2,0:T(8,128)(2,1)}, u32[]{:S(2)}) copy-start(bf16[2,704,64]{1,2,0:T(8,128)(2,1)} %param.11) | copy-start | bytes 540676
  43.3 4.0 %collective-permute-start = (f32[64,128]{1,0:T(8,128)S(1)}, f32[64,128]{1,0:T(8,128)S(1)}, u32[]{:S(2)}, u32[]{:S(2)}) collective-permute-start(f32[64,128]{1,0:T(8,128)S(1)} %fusion.13), channel_id=1, source_target_pairs={{0,1},{1,0},{2,3},{3,2},{4,5},{5,4},{6,7},{7,6},{8,9},{9,8},{10,11... | collective-permute-start | bytes 98312 | tf_op jit(solution)/shard_map/ppermute | solution.py:272
  48.1 4.9 %copy-start.3 = (bf16[64,768]{1,0:T(8,128)(2,1)S(1)}, bf16[64,768]{1,0:T(8,128)(2,1)}, u32[]{:S(2)}) copy-start(bf16[64,768]{1,0:T(8,128)(2,1)} %get-tuple-element.27) | copy-start | bytes 294916
  48.1 6.4 %copy-start.2 = (bf16[64,768]{1,0:T(8,128)(2,1)S(1)}, bf16[64,768]{1,0:T(8,128)(2,1)}, u32[]{:S(2)}) copy-start(bf16[64,768]{1,0:T(8,128)(2,1)} %get-tuple-element.28) | copy-start | bytes 294916
  48.1 8.8 %copy-start.1 = (bf16[64,768]{1,0:T(8,128)(2,1)S(1)}, bf16[64,768]{1,0:T(8,128)(2,1)}, u32[]{:S(2)}) copy-start(bf16[64,768]{1,0:T(8,128)(2,1)} %get-tuple-element.29) | copy-start | bytes 294916
  48.1 13.4 %all-to-all-start.2 = ((f16[16,72,128]{2,1,0:T(8,128)(2,1)}), f16[16,72,128]{2,1,0:T(8,128)(2,1)S(1)}, u32[]{:S(2)}, u32[]{:S(2)}) async-start(f16[16,72,128]{2,1,0:T(8,128)(2,1)} %broadcast_in_dim.16), calls=%async_computation.2 | async-start | bytes 589824 | tf_op jit(solution)/shard_map/all_to_all | solution.py:20
  53.0 8.7 %collective-permute-start.1 = (bf16[64,768]{1,0:T(8,128)(2,1)S(1)}, bf16[64,768]{1,0:T(8,128)(2,1)S(1)}, u32[]{:S(2)}, u32[]{:S(2)}) collective-permute-start(bf16[64,768]{1,0:T(8,128)(2,1)S(1)} %copy-done.3), channel_id=1, source_target_pairs={{0,8},{8,16},{16,24},{24,0},{1,9},{9,17},{17,25},{25,1},{2,10},{10... | collective-permute-start | bytes 294920 | tf_op jit(solution)/shard_map/ppermute | solution.py:240
  54.5 9.9 %collective-permute-start.2 = (bf16[64,768]{1,0:T(8,128)(2,1)S(1)}, bf16[64,768]{1,0:T(8,128)(2,1)S(1)}, u32[]{:S(2)}, u32[]{:S(2)}) collective-permute-start(bf16[64,768]{1,0:T(8,128)(2,1)S(1)} %copy-done.2), channel_id=1, source_target_pairs={{0,16},{8,24},{16,0},{24,8},{1,17},{9,25},{17,1},{25,9},{2,18},{10... | collective-permute-start | bytes 294920 | tf_op jit(solution)/shard_map/ppermute | solution.py:240
  56.9 7.5 %collective-permute-start.3 = (bf16[64,768]{1,0:T(8,128)(2,1)S(1)}, bf16[64,768]{1,0:T(8,128)(2,1)S(1)}, u32[]{:S(2)}, u32[]{:S(2)}) collective-permute-start(bf16[64,768]{1,0:T(8,128)(2,1)S(1)} %copy-done.1), channel_id=1, source_target_pairs={{0,24},{8,0},{16,8},{24,16},{1,25},{9,1},{17,9},{25,17},{2,26},{10... | collective-permute-start | bytes 294920 | tf_op jit(solution)/shard_map/ppermute | solution.py:240

commit v8 on v7

--- a/solution.py
+++ b/solution.py
@@ -73,9 +73,8 @@
     count, width = flat_ref.shape[:2]
     size = width // stage_ref.shape[0]
     for i in owners:
-        for j in range(count):
-            stage_ref[i, j * size : (j + 1) * size] = flat_ref[j, i * size : (i + 1) * size]
-        stage_ref[i, count * size : count * size + last.shape[0]] = last
+        rows = [flat_ref[j, i * size : (i + 1) * size] for j in range(count)]
+        stage_ref[i] = jnp.concatenate([*rows, last]).astype(bf16)
 
 
 def gain_lanes(gains):
@@ -95,7 +94,7 @@
 
 
 def first_kernel(*refs):
-    sources, (out_ref, flat_ref, stage_ref, tiles_ref, *held, in_sems, out_sems) = refs[:4], refs[4:]
+    sources, (out_ref, flat_ref, tiles_ref, *held, in_sems, out_sems) = refs[:4], refs[4:]
     pieces = [*sources[:2], sources[2].at[0], sources[3].at[0]]
     copies = [pltpu.make_async_copy(pieces[i], held[i], in_sems.at[i]) for i in range(4)]
     for copy in copies:
@@ -115,8 +114,7 @@
     writes = []
     for g in range(groups):
         part = slice(g * n // groups, (g + 1) * n // groups)
-        place(flat_ref, stage_ref, sums, range(part.start, part.stop))
-        tiles_ref[part] = stage_ref[part].astype(bf16)
+        place(flat_ref, tiles_ref, sums, range(part.start, part.stop))
         writes.append(pltpu.make_async_copy(tiles_ref.at[part], out_ref.at[part], out_sems.at[g]))
         writes[-1].start()
     for write in writes:
@@ -134,7 +132,6 @@
         out_specs=hbm,
         scratch_shapes=[
             pltpu.VMEM((2, width, ntok), f32),
-            pltpu.VMEM((n, rows, ntok), f32),
             pltpu.VMEM((n, rows, ntok), bf16),
             *[pltpu.VMEM(x.shape, x.dtype) for x in operands[:2]],
             *[pltpu.VMEM((count, width), bf16) for _ in range(2)],
@@ -199,7 +196,7 @@
 
 def second_kernel(*refs):
     branch_ref, mine_ref, side_ref, *other_refs = refs[:6]
-    out_ref, start_ref, gained_ref, last_ref, flat_ref, stage_ref = refs[6:]
+    out_ref, start_ref, gained_ref, last_ref, flat_ref = refs[6:]
     width, ntok = gained_ref.shape
     held, step = flat_ref.shape[1], mine_ref.shape[1] // 2
     sides = [side_ref[...], *[ref[:, 2 * step :] for ref in other_refs]]
@@ -218,8 +215,7 @@
         for k in range(2):
             weight = jnp.concatenate([ref[:, k * step : k * step + held] for ref in (mine_ref, *other_refs)])
             multiply(flat_ref, 2 * i + k, weight, columns)
-    place(flat_ref, stage_ref, sums, range(out_ref.shape[0]))
-    out_ref[...] = stage_ref[...].astype(bf16)
+    place(flat_ref, out_ref, sums, range(out_ref.shape[0]))
 
 
 def second_tiles(n, held, *operands):
@@ -231,7 +227,7 @@
         out_shape=[jax.ShapeDtypeStruct((n, rows, ntok), bf16), *[jax.ShapeDtypeStruct((width, ntok), f32)] * 3],
         in_specs=[vmem] * len(operands),
         out_specs=[vmem] * 4,
-        scratch_shapes=[pltpu.VMEM((4, held, ntok), f32), pltpu.VMEM((n, rows, ntok), f32)],
+        scratch_shapes=[pltpu.VMEM((4, held, ntok), f32)],
         compiler_params=pltpu.CompilerParams(vmem_limit_bytes=12 * 2**20),
     )(*operands)
 
@@ -270,8 +266,8 @@
     hidden = hidden_of(got[: 2 * size] * scale_in, None)
     part = down_project(down_now, hidden)
     part = part + lax.ppermute(part, "core", [(0, 1), (1, 0)])
-    parts = decoded(to_all(coded(part), ("y", "chip")))
-    parts = jnp.sum(parts.reshape(4, -1, width, ntok), axis=1)
+    parts = decoded(to_all(coded(part), ("chip", "y")))
+    parts = jnp.sum(parts.reshape(-1, 4, width, ntok), axis=0)
     parts = jnp.stack([parts[-i % 4] for i in range(8)])
     branch = lax.dynamic_slice_in_dim(parts, turn, 4).reshape(4 * width, ntok)
 

time: 116 us -> 116 us (level)
  no operation moved by 1% of the time
where the time goes in v8:
time: 116 us
  blocking collectives  64.2 us (55%)
  starting transfers between devices  25.1 us (22%)
  waiting for transfers between devices  16.9 us (15%)
  Pallas kernels  4.89 us (4%)
  local copies, waits for them, and re-layouts  2.7 us (2%)
  other arithmetic  1.17 us (1%)
    all_to_all x5, blocking collectives, exchange(): lax.all_to_all(tiles, axis, 0, 0, axis_index_groups=groups, tiled=True)  64.2 us
    all_to_all x2, starting transfers between devices, exchange(): lax.all_to_all(tiles, axis, 0, 0, axis_index_groups=groups, tiled=True)  16.9 us
    all_to_all x2, waiting for transfers between devices, exchange(): lax.all_to_all(tiles, axis, 0, 0, axis_index_groups=groups, tiled=True)  13 us
    ppermute x3, starting transfers between devices, handed(): return lax.ppermute(array, 'y', [(i, (i + d) % 4) for i in range(4)])  5.01 us
    ppermute x1, starting transfers between devices, sublayers(): part = part + lax.ppermute(part, 'core', [(0, 1), (1, 0)])  3.14 us
    ppermute x3, waiting for transfers between devices, handed(): return lax.ppermute(array, 'y', [(i, (i + d) % 4) for i in range(4)])  3.08 us
  transfers between devices with their start and end apart: 6, of which 4 were waited for; matrix products, arithmetic and copies ran while one was open for 2% of the time, Pallas kernels for 2%

profile of v8, /device:TPU:1, one launch (start us, length us, event | category | flops | bytes accessed | tf_op | source)
XLA Modules:
  0.0 115.6 jit_solution(13202087088578640857)
XLA Ops:
  0.0 2.2 %shard_map.64 = bf16[32,48,128]{2,1,0:T(8,128)(2,1)} custom-call(bf16[64,128]{1,0:T(8,128)(2,1)} %bitcast.32, f32[2,64]{1,0:T(2,128)} %refs_1_.3, bf16[2,64,704]{2,1,0:T(8,128)(2,1)} %refs_3_.3, bf16[2,64,704]{2,1,0:T(8,128)(2,1)} %refs_4_.1), custom_call_target="tpu_custom_call" | custom-call | tf_op jit(solution)/shard_map/pallas_call | solution.py:128
  2.2 12.0 %all-to-all-start = ((bf16[32,48,128]{2,1,0:T(8,128)(2,1)}), bf16[32,48,128]{2,1,0:T(8,128)(2,1)S(1)}, u32[]{:S(2)}, u32[]{:S(2)}) async-start(bf16[32,48,128]{2,1,0:T(8,128)(2,1)} %shard_map.64), calls=%async_computation | async-start | bytes 786432 | tf_op jit(solution)/shard_map/all_to_all | solution.py:20
  14.3 2.0 %shard_map.65 = (bf16[64,768]{1,0:T(8,128)(2,1)}, bf16[64,768]{1,0:T(8,128)(2,1)}, bf16[64,768]{1,0:T(8,128)(2,1)}, bf16[64,768]{1,0:T(8,128)(2,1)}) custom-call(bf16[64,128]{1,0:T(8,128)(2,1)} %bitcast.33, f32[2,64]{1,0:T(2,128)} %refs_1_.3, f32[2,64]{1,0:T(2,128)} %refs_2_.3, bf16[2,64,704]{2,1,0:T(8,128)(2,1)} %refs_3_.3, bf16[2,64,704]{2,1,0:T(8,128)(2,1)} %refs_4_.1), custom_call_target="tpu_custom_call" | custom-call | tf_op jit(solution)/shard_map/pallas_call | solution.py:181
  16.3 0.0 copy-start
  16.3 0.8 slice.80.refs_2_
  17.1 0.8 slice.79.refs_1_
  18.0 0.0 copy-done
  18.0 10.1 %all-to-all-done = bf16[32,48,128]{2,1,0:T(8,128)(2,1)S(1)} async-done(((bf16[32,48,128]{2,1,0:T(8,128)(2,1)}), bf16[32,48,128]{2,1,0:T(8,128)(2,1)S(1)}, u32[]{:S(2)}, u32[]{:S(2)}) %all-to-all-start) | async-done | bytes 393248 | tf_op jit(solution)/shard_map/all_to_all | solution.py:20
  28.1 0.1 convert_reduce_fusion
  28.3 14.8 %all_to_all.35 = bf16[32,22,128]{2,1,0:T(8,128)(2,1)S(1)} all-to-all(bf16[32,22,128]{2,1,0:T(8,128)(2,1)S(1)} %broadcast_in_dim.14), channel_id=1, replica_groups=mesh['z'=8,'y'=4,'chip'=4,'core'=2] {'z','y'}, dimensions={0} | all-to-all | bytes 360448 | tf_op jit(solution)/shard_map/all_to_all | solution.py:20
  43.0 0.1 reshape.120
  43.1 0.2 fusion.13
  43.3 3.1 %collective-permute-start = (f32[64,128]{1,0:T(8,128)S(1)}, f32[64,128]{1,0:T(8,128)S(1)}, u32[]{:S(2)}, u32[]{:S(2)}) collective-permute-start(f32[64,128]{1,0:T(8,128)S(1)} %fusion.13), channel_id=1, source_target_pairs={{0,1},{1,0},{2,3},{3,2},{4,5},{5,4},{6,7},{7,6},{8,9},{9,8},{10,11... | collective-permute-start | bytes 98312 | tf_op jit(solution)/shard_map/ppermute | solution.py:268
  46.4 0.9 collective-permute-done
  47.3 0.7 broadcast_in_dim.16
  48.1 0.0 copy-start.3
  48.1 0.0 copy-start.2
  48.1 0.0 copy-start.1
  48.1 4.9 %all-to-all-start.2 = ((f16[16,72,128]{2,1,0:T(8,128)(2,1)}), f16[16,72,128]{2,1,0:T(8,128)(2,1)S(1)}, u32[]{:S(2)}, u32[]{:S(2)}) async-start(f16[16,72,128]{2,1,0:T(8,128)(2,1)} %broadcast_in_dim.16), calls=%async_computation.2 | async-start | bytes 589824 | tf_op jit(solution)/shard_map/all_to_all | solution.py:20
  53.0 0.0 copy-done.3
  53.0 1.4 %collective-permute-start.1 = (bf16[64,768]{1,0:T(8,128)(2,1)S(1)}, bf16[64,768]{1,0:T(8,128)(2,1)S(1)}, u32[]{:S(2)}, u32[]{:S(2)}) collective-permute-start(bf16[64,768]{1,0:T(8,128)(2,1)S(1)} %copy-done.3), channel_id=1, source_target_pairs={{0,8},{8,16},{16,24},{24,0},{1,9},{9,17},{17,25},{25,1},{2,10},{10... | collective-permute-start | bytes 294920 | tf_op jit(solution)/shard_map/ppermute | solution.py:236
  54.4 0.0 copy-done.2
  54.5 2.4 %collective-permute-start.2 = (bf16[64,768]{1,0:T(8,128)(2,1)S(1)}, bf16[64,768]{1,0:T(8,128)(2,1)S(1)}, u32[]{:S(2)}, u32[]{:S(2)}) collective-permute-start(bf16[64,768]{1,0:T(8,128)(2,1)S(1)} %copy-done.2), channel_id=1, source_target_pairs={{0,16},{8,24},{16,0},{24,8},{1,17},{9,25},{17,1},{25,9},{2,18},{10... | collective-permute-start | bytes 294920 | tf_op jit(solution)/shard_map/ppermute | solution.py:236
  56.8 0.0 copy-done.1
  56.8 1.2 %collective-permute-start.3 = (bf16[64,768]{1,0:T(8,128)(2,1)S(1)}, bf16[64,768]{1,0:T(8,128)(2,1)S(1)}, u32[]{:S(2)}, u32[]{:S(2)}) collective-permute-start(bf16[64,768]{1,0:T(8,128)(2,1)S(1)} %copy-done.1), channel_id=1, source_target_pairs={{0,24},{8,0},{16,8},{24,16},{1,25},{9,1},{17,9},{25,17},{2,26},{10... | collective-permute-start | bytes 294920 | tf_op jit(solution)/shard_map/ppermute | solution.py:236
  58.0 2.9 %all-to-all-done.2 = f16[16,72,128]{2,1,0:T(8,128)(2,1)S(1)} async-done(((f16[16,72,128]{2,1,0:T(8,128)(2,1)}), f16[16,72,128]{2,1,0:T(8,128)(2,1)S(1)}, u32[]{:S(2)}, u32[]{:S(2)}) %all-to-all-start.2) | async-done | bytes 294944 | tf_op jit(solution)/shard_map/all_to_all | solution.py:20
  61.2 0.0 collective-permute-done.1.refs_3_
  61.2 3.1 %collective-permute-done.2.refs_4_ = bf16[64,768]{1,0:T(8,128)(2,1)S(1)} collective-permute-done((bf16[64,768]{1,0:T(8,128)(2,1)S(1)}, bf16[64,768]{1,0:T(8,128)(2,1)S(1)}, u32[]{:S(2)}, u32[]{:S(2)}) %collective-permute-start.2) | collective-permute-done | bytes 98336 | tf_op jit(solution)/shard_map/ppermute | solution.py:236
  64.3 0.0 collective-permute-done.3.refs_5_
  64.3 0.6 shard_map.66
  64.9 11.1 %all_to_all.36 = bf16[8,96,128]{2,1,0:T(8,128)(2,1)S(1)} all-to-all(bf16[8,96,128]{2,1,0:T(8,128)(2,1)S(1)} %get-tuple-element.32), channel_id=1, replica_groups=mesh['z'=8,'y'=4,'chip'=4,'core'=2] {'z'}, dimensions={0} | all-to-all | bytes 393216 | tf_op jit(solution)/shard_map/all_to_all | solution.py:20
  76.1 14.6 %all_to_all.37 = bf16[32,22,128]{2,1,0:T(8,128)(2,1)S(1)} all-to-all(bf16[32,22,128]{2,1,0:T(8,128)(2,1)S(1)} %broadcast_in_dim.17), channel_id=1, replica_groups={{0,32,64,96,128,160,192,224,8,40,72,104,136,168,200,232,16,48,80,112,14..., dimensions={0} | all-to-all | bytes 360448 | tf_op jit(solution)/shard_map/all_to_all | solution.py:20
  90.8 0.1 reshape.123
  90.8 0.2 abs_reduce_fusion
  91.1 11.5 %all_to_all.38 = f16[8,72,128]{2,1,0:T(8,128)(2,1)S(1)} all-to-all(f16[8,72,128]{2,1,0:T(8,128)(2,1)S(1)} %broadcast_in_dim.19), channel_id=1, replica_groups=mesh['z'=8,'y'=4,'chip'=4,'core'=2] {'chip','core'}, dimensions={0} | all-to-all | bytes 294912 | tf_op jit(solution)/shard_map/all_to_all | solution.py:20
  102.7 12.2 %all_to_all.39 = f32[32,1,128]{2,1,0:T(1,128)S(1)} all-to-all(f32[32,1,128]{2,1,0:T(1,128)S(1)} %broadcast_in_dim.20), channel_id=1, replica_groups=mesh['z'=8,'y'=4,'chip'=4,'core'=2] {'z','y'}, dimensions={0} | all-to-all | bytes 32768 | tf_op jit(solution)/shard_map/all_to_all | solution.py:20
  114.9 0.6 fusion.3
  (42 shorter events, 0.7 us)
Async XLA Ops:
  2.2 25.9 %all-to-all-start = ((bf16[32,48,128]{2,1,0:T(8,128)(2,1)}), bf16[32,48,128]{2,1,0:T(8,128)(2,1)S(1)}, u32[]{:S(2)}, u32[]{:S(2)}) async-start(bf16[32,48,128]{2,1,0:T(8,128)(2,1)} %shard_map.64), calls=%async_computation | async-start | bytes 786432 | tf_op jit(solution)/shard_map/all_to_all | solution.py:20
  16.3 1.7 %copy-start = (bf16[2,704,64]{1,2,0:T(8,128)(2,1)S(1)}, bf16[2,704,64]{1,2,0:T(8,128)(2,1)}, u32[]{:S(2)}) copy-start(bf16[2,704,64]{1,2,0:T(8,128)(2,1)} %param.11) | copy-start | bytes 540676
  43.3 4.0 %collective-permute-start = (f32[64,128]{1,0:T(8,128)S(1)}, f32[64,128]{1,0:T(8,128)S(1)}, u32[]{:S(2)}, u32[]{:S(2)}) collective-permute-start(f32[64,128]{1,0:T(8,128)S(1)} %fusion.13), channel_id=1, source_target_pairs={{0,1},{1,0},{2,3},{3,2},{4,5},{5,4},{6,7},{7,6},{8,9},{9,8},{10,11... | collective-permute-start | bytes 98312 | tf_op jit(solution)/shard_map/ppermute | solution.py:268
  48.1 4.9 %copy-start.3 = (bf16[64,768]{1,0:T(8,128)(2,1)S(1)}, bf16[64,768]{1,0:T(8,128)(2,1)}, u32[]{:S(2)}) copy-start(bf16[64,768]{1,0:T(8,128)(2,1)} %get-tuple-element.27) | copy-start | bytes 294916
  48.1 6.4 %copy-start.2 = (bf16[64,768]{1,0:T(8,128)(2,1)S(1)}, bf16[64,768]{1,0:T(8,128)(2,1)}, u32[]{:S(2)}) copy-start(bf16[64,768]{1,0:T(8,128)(2,1)} %get-tuple-element.28) | copy-start | bytes 294916
  48.1 8.8 %copy-start.1 = (bf16[64,768]{1,0:T(8,128)(2,1)S(1)}, bf16[64,768]{1,0:T(8,128)(2,1)}, u32[]{:S(2)}) copy-start(bf16[64,768]{1,0:T(8,128)(2,1)} %get-tuple-element.29) | copy-start | bytes 294916
  48.1 12.8 %all-to-all-start.2 = ((f16[16,72,128]{2,1,0:T(8,128)(2,1)}), f16[16,72,128]{2,1,0:T(8,128)(2,1)S(1)}, u32[]{:S(2)}, u32[]{:S(2)}) async-start(f16[16,72,128]{2,1,0:T(8,128)(2,1)} %broadcast_in_dim.16), calls=%async_computation.2 | async-start | bytes 589824 | tf_op jit(solution)/shard_map/all_to_all | solution.py:20
  53.0 8.2 %collective-permute-start.1 = (bf16[64,768]{1,0:T(8,128)(2,1)S(1)}, bf16[64,768]{1,0:T(8,128)(2,1)S(1)}, u32[]{:S(2)}, u32[]{:S(2)}) collective-permute-start(bf16[64,768]{1,0:T(8,128)(2,1)S(1)} %copy-done.3), channel_id=1, source_target_pairs={{0,8},{8,16},{16,24},{24,0},{1,9},{9,17},{17,25},{25,1},{2,10},{10... | collective-permute-start | bytes 294920 | tf_op jit(solution)/shard_map/ppermute | solution.py:236
  54.5 9.8 %collective-permute-start.2 = (bf16[64,768]{1,0:T(8,128)(2,1)S(1)}, bf16[64,768]{1,0:T(8,128)(2,1)S(1)}, u32[]{:S(2)}, u32[]{:S(2)}) collective-permute-start(bf16[64,768]{1,0:T(8,128)(2,1)S(1)} %copy-done.2), channel_id=1, source_target_pairs={{0,16},{8,24},{16,0},{24,8},{1,17},{9,25},{17,1},{25,9},{2,18},{10... | collective-permute-start | bytes 294920 | tf_op jit(solution)/shard_map/ppermute | solution.py:236
  56.8 7.4 %collective-permute-start.3 = (bf16[64,768]{1,0:T(8,128)(2,1)S(1)}, bf16[64,768]{1,0:T(8,128)(2,1)S(1)}, u32[]{:S(2)}, u32[]{:S(2)}) collective-permute-start(bf16[64,768]{1,0:T(8,128)(2,1)S(1)} %copy-done.1), channel_id=1, source_target_pairs={{0,24},{8,0},{16,8},{24,16},{1,25},{9,1},{17,9},{25,17},{2,26},{10... | collective-permute-start | bytes 294920 | tf_op jit(solution)/shard_map/ppermute | solution.py:236

commit v9 on v7

--- a/solution.py
+++ b/solution.py
@@ -125,7 +125,7 @@
 
 def first_tiles(n, *operands):
     (count, ntok), width = operands[0].shape, operands[-1].shape[2]
-    rows, groups = 2 * (width // n) + 4, 2
+    rows, groups = 2 * (width // n) + 4, 4
     hbm = pl.BlockSpec(memory_space=pltpu.HBM)
     return pl.pallas_call(
         first_kernel,
@@ -270,8 +270,8 @@
     hidden = hidden_of(got[: 2 * size] * scale_in, None)
     part = down_project(down_now, hidden)
     part = part + lax.ppermute(part, "core", [(0, 1), (1, 0)])
-    parts = decoded(to_all(coded(part), ("y", "chip")))
-    parts = jnp.sum(parts.reshape(4, -1, width, ntok), axis=1)
+    parts = decoded(to_all(coded(part), ("chip", "y")))
+    parts = jnp.sum(parts.reshape(-1, 4, width, ntok), axis=0)
     parts = jnp.stack([parts[-i % 4] for i in range(8)])
     branch = lax.dynamic_slice_in_dim(parts, turn, 4).reshape(4 * width, ntok)
 

time: 116 us -> 116 us (level)
  no operation moved by 1% of the time
where the time goes in v9:
time: 116 us
  blocking collectives  64.2 us (55%)
  starting transfers between devices  25.1 us (22%)
  waiting for transfers between devices  16.9 us (15%)
  Pallas kernels  4.92 us (4%)
  local copies, waits for them, and re-layouts  2.7 us (2%)
  other arithmetic  1.17 us (1%)
    all_to_all x5, blocking collectives, exchange(): lax.all_to_all(tiles, axis, 0, 0, axis_index_groups=groups, tiled=True)  64.2 us
    all_to_all x2, starting transfers between devices, exchange(): lax.all_to_all(tiles, axis, 0, 0, axis_index_groups=groups, tiled=True)  16.9 us
    all_to_all x2, waiting for transfers between devices, exchange(): lax.all_to_all(tiles, axis, 0, 0, axis_index_groups=groups, tiled=True)  13 us
    ppermute x3, starting transfers between devices, handed(): return lax.ppermute(array, 'y', [(i, (i + d) % 4) for i in range(4)])  5.01 us
    ppermute x1, starting transfers between devices, sublayers(): part = part + lax.ppermute(part, 'core', [(0, 1), (1, 0)])  3.14 us
    ppermute x3, waiting for transfers between devices, handed(): return lax.ppermute(array, 'y', [(i, (i + d) % 4) for i in range(4)])  3.08 us
  transfers between devices with their start and end apart: 6, of which 4 were waited for; matrix products, arithmetic and copies ran while one was open for 2% of the time, Pallas kernels for 2%

profile of v9, /device:TPU:1, one launch (start us, length us, event | category | flops | bytes accessed | tf_op | source)
XLA Modules:
  0.0 115.6 jit_solution(14925404622049347062)
XLA Ops:
  0.0 2.2 %shard_map.64 = bf16[32,48,128]{2,1,0:T(8,128)(2,1)} custom-call(bf16[64,128]{1,0:T(8,128)(2,1)} %bitcast.32, f32[2,64]{1,0:T(2,128)} %refs_1_.3, bf16[2,64,704]{2,1,0:T(8,128)(2,1)} %refs_3_.3, bf16[2,64,704]{2,1,0:T(8,128)(2,1)} %refs_4_.1), custom_call_target="tpu_custom_call" | custom-call | tf_op jit(solution)/shard_map/pallas_call | solution.py:130
  2.2 12.0 %all-to-all-start = ((bf16[32,48,128]{2,1,0:T(8,128)(2,1)}), bf16[32,48,128]{2,1,0:T(8,128)(2,1)S(1)}, u32[]{:S(2)}, u32[]{:S(2)}) async-start(bf16[32,48,128]{2,1,0:T(8,128)(2,1)} %shard_map.64), calls=%async_computation | async-start | bytes 786432 | tf_op jit(solution)/shard_map/all_to_all | solution.py:20
  14.3 2.0 %shard_map.65 = (bf16[64,768]{1,0:T(8,128)(2,1)}, bf16[64,768]{1,0:T(8,128)(2,1)}, bf16[64,768]{1,0:T(8,128)(2,1)}, bf16[64,768]{1,0:T(8,128)(2,1)}) custom-call(bf16[64,128]{1,0:T(8,128)(2,1)} %bitcast.33, f32[2,64]{1,0:T(2,128)} %refs_1_.3, f32[2,64]{1,0:T(2,128)} %refs_2_.3, bf16[2,64,704]{2,1,0:T(8,128)(2,1)} %refs_3_.3, bf16[2,64,704]{2,1,0:T(8,128)(2,1)} %refs_4_.1), custom_call_target="tpu_custom_call" | custom-call | tf_op jit(solution)/shard_map/pallas_call | solution.py:184
  16.3 0.0 copy-start
  16.3 0.8 slice.80.refs_2_
  17.1 0.8 slice.79.refs_1_
  18.0 0.0 copy-done
  18.0 10.1 %all-to-all-done = bf16[32,48,128]{2,1,0:T(8,128)(2,1)S(1)} async-done(((bf16[32,48,128]{2,1,0:T(8,128)(2,1)}), bf16[32,48,128]{2,1,0:T(8,128)(2,1)S(1)}, u32[]{:S(2)}, u32[]{:S(2)}) %all-to-all-start) | async-done | bytes 393248 | tf_op jit(solution)/shard_map/all_to_all | solution.py:20
  28.1 0.1 convert_reduce_fusion
  28.3 14.8 %all_to_all.35 = bf16[32,22,128]{2,1,0:T(8,128)(2,1)S(1)} all-to-all(bf16[32,22,128]{2,1,0:T(8,128)(2,1)S(1)} %broadcast_in_dim.14), channel_id=1, replica_groups=mesh['z'=8,'y'=4,'chip'=4,'core'=2] {'z','y'}, dimensions={0} | all-to-all | bytes 360448 | tf_op jit(solution)/shard_map/all_to_all | solution.py:20
  43.0 0.1 reshape.120
  43.1 0.2 fusion.13
  43.3 3.1 %collective-permute-start = (f32[64,128]{1,0:T(8,128)S(1)}, f32[64,128]{1,0:T(8,128)S(1)}, u32[]{:S(2)}, u32[]{:S(2)}) collective-permute-start(f32[64,128]{1,0:T(8,128)S(1)} %fusion.13), channel_id=1, source_target_pairs={{0,1},{1,0},{2,3},{3,2},{4,5},{5,4},{6,7},{7,6},{8,9},{9,8},{10,11... | collective-permute-start | bytes 98312 | tf_op jit(solution)/shard_map/ppermute | solution.py:272
  46.4 0.9 collective-permute-done
  47.3 0.7 broadcast_in_dim.16
  48.1 0.0 copy-start.3
  48.1 0.0 copy-start.2
  48.1 0.0 copy-start.1
  48.1 4.9 %all-to-all-start.2 = ((f16[16,72,128]{2,1,0:T(8,128)(2,1)}), f16[16,72,128]{2,1,0:T(8,128)(2,1)S(1)}, u32[]{:S(2)}, u32[]{:S(2)}) async-start(f16[16,72,128]{2,1,0:T(8,128)(2,1)} %broadcast_in_dim.16), calls=%async_computation.2 | async-start | bytes 589824 | tf_op jit(solution)/shard_map/all_to_all | solution.py:20
  53.0 0.0 copy-done.3
  53.0 1.4 %collective-permute-start.1 = (bf16[64,768]{1,0:T(8,128)(2,1)S(1)}, bf16[64,768]{1,0:T(8,128)(2,1)S(1)}, u32[]{:S(2)}, u32[]{:S(2)}) collective-permute-start(bf16[64,768]{1,0:T(8,128)(2,1)S(1)} %copy-done.3), channel_id=1, source_target_pairs={{0,8},{8,16},{16,24},{24,0},{1,9},{9,17},{17,25},{25,1},{2,10},{10... | collective-permute-start | bytes 294920 | tf_op jit(solution)/shard_map/ppermute | solution.py:240
  54.5 0.0 copy-done.2
  54.5 2.4 %collective-permute-start.2 = (bf16[64,768]{1,0:T(8,128)(2,1)S(1)}, bf16[64,768]{1,0:T(8,128)(2,1)S(1)}, u32[]{:S(2)}, u32[]{:S(2)}) collective-permute-start(bf16[64,768]{1,0:T(8,128)(2,1)S(1)} %copy-done.2), channel_id=1, source_target_pairs={{0,16},{8,24},{16,0},{24,8},{1,17},{9,25},{17,1},{25,9},{2,18},{10... | collective-permute-start | bytes 294920 | tf_op jit(solution)/shard_map/ppermute | solution.py:240
  56.8 0.0 copy-done.1
  56.9 1.2 %collective-permute-start.3 = (bf16[64,768]{1,0:T(8,128)(2,1)S(1)}, bf16[64,768]{1,0:T(8,128)(2,1)S(1)}, u32[]{:S(2)}, u32[]{:S(2)}) collective-permute-start(bf16[64,768]{1,0:T(8,128)(2,1)S(1)} %copy-done.1), channel_id=1, source_target_pairs={{0,24},{8,0},{16,8},{24,16},{1,25},{9,1},{17,9},{25,17},{2,26},{10... | collective-permute-start | bytes 294920 | tf_op jit(solution)/shard_map/ppermute | solution.py:240
  58.0 2.9 %all-to-all-done.2 = f16[16,72,128]{2,1,0:T(8,128)(2,1)S(1)} async-done(((f16[16,72,128]{2,1,0:T(8,128)(2,1)}), f16[16,72,128]{2,1,0:T(8,128)(2,1)S(1)}, u32[]{:S(2)}, u32[]{:S(2)}) %all-to-all-start.2) | async-done | bytes 294944 | tf_op jit(solution)/shard_map/all_to_all | solution.py:20
  61.2 0.0 collective-permute-done.1.refs_3_
  61.2 3.1 %collective-permute-done.2.refs_4_ = bf16[64,768]{1,0:T(8,128)(2,1)S(1)} collective-permute-done((bf16[64,768]{1,0:T(8,128)(2,1)S(1)}, bf16[64,768]{1,0:T(8,128)(2,1)S(1)}, u32[]{:S(2)}, u32[]{:S(2)}) %collective-permute-start.2) | collective-permute-done | bytes 98336 | tf_op jit(solution)/shard_map/ppermute | solution.py:240
  64.3 0.0 collective-permute-done.3.refs_5_
  64.3 0.6 shard_map.66
  64.9 11.1 %all_to_all.36 = bf16[8,96,128]{2,1,0:T(8,128)(2,1)S(1)} all-to-all(bf16[8,96,128]{2,1,0:T(8,128)(2,1)S(1)} %get-tuple-element.32), channel_id=1, replica_groups=mesh['z'=8,'y'=4,'chip'=4,'core'=2] {'z'}, dimensions={0} | all-to-all | bytes 393216 | tf_op jit(solution)/shard_map/all_to_all | solution.py:20
  76.2 14.6 %all_to_all.37 = bf16[32,22,128]{2,1,0:T(8,128)(2,1)S(1)} all-to-all(bf16[32,22,128]{2,1,0:T(8,128)(2,1)S(1)} %broadcast_in_dim.17), channel_id=1, replica_groups={{0,32,64,96,128,160,192,224,8,40,72,104,136,168,200,232,16,48,80,112,14..., dimensions={0} | all-to-all | bytes 360448 | tf_op jit(solution)/shard_map/all_to_all | solution.py:20
  90.8 0.1 reshape.123
  90.9 0.2 abs_reduce_fusion
  91.1 11.5 %all_to_all.38 = f16[8,72,128]{2,1,0:T(8,128)(2,1)S(1)} all-to-all(f16[8,72,128]{2,1,0:T(8,128)(2,1)S(1)} %broadcast_in_dim.19), channel_id=1, replica_groups=mesh['z'=8,'y'=4,'chip'=4,'core'=2] {'chip','core'}, dimensions={0} | all-to-all | bytes 294912 | tf_op jit(solution)/shard_map/all_to_all | solution.py:20
  102.8 12.2 %all_to_all.39 = f32[32,1,128]{2,1,0:T(1,128)S(1)} all-to-all(f32[32,1,128]{2,1,0:T(1,128)S(1)} %broadcast_in_dim.20), channel_id=1, replica_groups=mesh['z'=8,'y'=4,'chip'=4,'core'=2] {'z','y'}, dimensions={0} | all-to-all | bytes 32768 | tf_op jit(solution)/shard_map/all_to_all | solution.py:20
  115.0 0.6 fusion.3
  (42 shorter events, 0.7 us)
Async XLA Ops:
  2.2 25.9 %all-to-all-start = ((bf16[32,48,128]{2,1,0:T(8,128)(2,1)}), bf16[32,48,128]{2,1,0:T(8,128)(2,1)S(1)}, u32[]{:S(2)}, u32[]{:S(2)}) async-start(bf16[32,48,128]{2,1,0:T(8,128)(2,1)} %shard_map.64), calls=%async_computation | async-start | bytes 786432 | tf_op jit(solution)/shard_map/all_to_all | solution.py:20
  16.3 1.7 %copy-start = (bf16[2,704,64]{1,2,0:T(8,128)(2,1)S(1)}, bf16[2,704,64]{1,2,0:T(8,128)(2,1)}, u32[]{:S(2)}) copy-start(bf16[2,704,64]{1,2,0:T(8,128)(2,1)} %param.11) | copy-start | bytes 540676
  43.3 4.0 %collective-permute-start = (f32[64,128]{1,0:T(8,128)S(1)}, f32[64,128]{1,0:T(8,128)S(1)}, u32[]{:S(2)}, u32[]{:S(2)}) collective-permute-start(f32[64,128]{1,0:T(8,128)S(1)} %fusion.13), channel_id=1, source_target_pairs={{0,1},{1,0},{2,3},{3,2},{4,5},{5,4},{6,7},{7,6},{8,9},{9,8},{10,11... | collective-permute-start | bytes 98312 | tf_op jit(solution)/shard_map/ppermute | solution.py:272
  48.1 4.9 %copy-start.3 = (bf16[64,768]{1,0:T(8,128)(2,1)S(1)}, bf16[64,768]{1,0:T(8,128)(2,1)}, u32[]{:S(2)}) copy-start(bf16[64,768]{1,0:T(8,128)(2,1)} %get-tuple-element.27) | copy-start | bytes 294916
  48.1 6.4 %copy-start.2 = (bf16[64,768]{1,0:T(8,128)(2,1)S(1)}, bf16[64,768]{1,0:T(8,128)(2,1)}, u32[]{:S(2)}) copy-start(bf16[64,768]{1,0:T(8,128)(2,1)} %get-tuple-element.28) | copy-start | bytes 294916
  48.1 8.8 %copy-start.1 = (bf16[64,768]{1,0:T(8,128)(2,1)S(1)}, bf16[64,768]{1,0:T(8,128)(2,1)}, u32[]{:S(2)}) copy-start(bf16[64,768]{1,0:T(8,128)(2,1)} %get-tuple-element.29) | copy-start | bytes 294916
  48.1 12.8 %all-to-all-start.2 = ((f16[16,72,128]{2,1,0:T(8,128)(2,1)}), f16[16,72,128]{2,1,0:T(8,128)(2,1)S(1)}, u32[]{:S(2)}, u32[]{:S(2)}) async-start(f16[16,72,128]{2,1,0:T(8,128)(2,1)} %broadcast_in_dim.16), calls=%async_computation.2 | async-start | bytes 589824 | tf_op jit(solution)/shard_map/all_to_all | solution.py:20
  53.0 8.2 %collective-permute-start.1 = (bf16[64,768]{1,0:T(8,128)(2,1)S(1)}, bf16[64,768]{1,0:T(8,128)(2,1)S(1)}, u32[]{:S(2)}, u32[]{:S(2)}) collective-permute-start(bf16[64,768]{1,0:T(8,128)(2,1)S(1)} %copy-done.3), channel_id=1, source_target_pairs={{0,8},{8,16},{16,24},{24,0},{1,9},{9,17},{17,25},{25,1},{2,10},{10... | collective-permute-start | bytes 294920 | tf_op jit(solution)/shard_map/ppermute | solution.py:240
  54.5 9.8 %collective-permute-start.2 = (bf16[64,768]{1,0:T(8,128)(2,1)S(1)}, bf16[64,768]{1,0:T(8,128)(2,1)S(1)}, u32[]{:S(2)}, u32[]{:S(2)}) collective-permute-start(bf16[64,768]{1,0:T(8,128)(2,1)S(1)} %copy-done.2), channel_id=1, source_target_pairs={{0,16},{8,24},{16,0},{24,8},{1,17},{9,25},{17,1},{25,9},{2,18},{10... | collective-permute-start | bytes 294920 | tf_op jit(solution)/shard_map/ppermute | solution.py:240
  56.9 7.4 %collective-permute-start.3 = (bf16[64,768]{1,0:T(8,128)(2,1)S(1)}, bf16[64,768]{1,0:T(8,128)(2,1)S(1)}, u32[]{:S(2)}, u32[]{:S(2)}) collective-permute-start(bf16[64,768]{1,0:T(8,128)(2,1)S(1)} %copy-done.1), channel_id=1, source_target_pairs={{0,24},{8,0},{16,8},{24,16},{1,25},{9,1},{17,9},{25,17},{2,26},{10... | collective-permute-start | bytes 294920 | tf_op jit(solution)/shard_map/ppermute | solution.py:240
